TPU v7x, 32 devices: a whole 2x2x4 slice. The times are simulated.
32 devices in a mesh: fs: 16 (over z, y, x), tp: 2 (over core).
Axes of the slice: x: 2, y: 2, z: 4, core: 2. Of those that a mesh axis runs over, the one named last changes fastest.
Arguments:
- x_late: bfloat16 [4096, 2048], P('fs'), may hold values from -6 to 6
- x_early: bfloat16 [4096, 2048], P('fs'), may hold values from -6 to 6
- cotangent: bfloat16 [4096, 2048], P('fs'), may hold values from -6 to 6
- w_gate: bfloat16 [2048, 4096], P('fs', 'tp'), may hold values from -0.125 to 0.125
- w_up: bfloat16 [2048, 4096], P('fs', 'tp'), may hold values from -0.125 to 0.125
- w_down: bfloat16 [4096, 2048], P('tp', 'fs'), may hold values from -0.09375 to 0.09375
- conv_taps: float32 [3, 4096], replicated, may hold values from -3 to 3
- conv_bias: float32 [4096], replicated, may hold values from -3 to 3
- grad_down: float32 [4096, 2048], P('tp', 'fs'), may hold values from -60 to 60
Outputs:
- y_late: bfloat16 [4096, 2048], P('fs')
- dx_early: bfloat16 [4096, 2048], P('fs')
- grad_down_out: float32 [4096, 2048], P('tp', 'fs')
All inputs are finite; a program needn't handle non-finite values.
Results may differ from a plain program's by a relative error of at most 0.017.
Values may be sent and summed in bfloat16 or wider, within the bound.
A program may use at most 128 MiB of HBM per device.

v0:
```python
import functools

import jax
import jax.numpy as jnp
from jax import lax
from jax.experimental import pallas as pl
from jax.experimental.pallas import tpu as pltpu
from jax.sharding import PartitionSpec as P

GROUP = 4
VMEM_BYTES = 60 * 1024 * 1024
VMEM = pl.BlockSpec(memory_space=pltpu.VMEM)


def place():
    f, c = lax.axis_index("fs"), lax.axis_index("tp")
    q, z = lax.rem(f, GROUP), lax.div(f, GROUP)
    qx = q + 1 - 2 * lax.rem(q, 2)
    qy = q + 2 - 4 * lax.div(q, 2)
    qa, qb = qx + c * (qy - qx), qy + c * (qx - qy)
    return f, c, q, z, qa, qb, GROUP - 1 - q


def at(start, size):
    return pl.ds(pl.multiple_of(start, size), size)


def remote(src, dst, send, recv, **device):
    return pltpu.make_async_remote_copy(
        src_ref=src, dst_ref=dst, send_sem=send, recv_sem=recv,
        device_id=device, device_id_type=pl.DeviceIdType.MESH,
    )


def total(dst, srcs, rows, step=16):
    @pl.loop(0, rows, step=step)
    def _(i):
        sl = pl.ds(pl.multiple_of(i, step), step)
        out = srcs[0][sl, :].astype(jnp.float32)
        for s in srcs[1:]:
            out = out + s[sl, :].astype(jnp.float32)
        dst[sl, :] = out.astype(dst.dtype)


def mm(left, right, dims=((1,), (0,))):
    return lax.dot_general(left, right, (dims, ((), ())), preferred_element_type=jnp.float32)


def layer_kernel(nz, tile, x0, x1, x2, wg, wu, wd, taps, bias, y, dx, g,
                 t0, t1, t2, og, ou, od, hid, hid_t, conv_s, up_s, dup, dgate, yp, xp, gp,
                 core, summed, got, gin, gsum,
                 loc, w_s, w_r, n_s, n_r, p_s, p_r, r_s, r_r, l_s, l_r,
                 c_s, c_r, a_s, a_r, z_s, z_r, g_s, g_r, e_s, e_r):
    f, c, q, z, qa, qb, qd = place()
    base = z * GROUP
    xs, ts, outs = (x0, x1, x2), (t0, t1, t2), (og, ou, od)
    rows, d_model = x0.shape
    half = rows // 2
    r, u = wg.shape[0], og.shape[1]
    wide = GROUP * r
    first, last = z > 0, z < nz - 1

    barrier = pltpu.get_barrier_semaphore()
    for peer in (qa, qb, qd):
        pl.semaphore_signal(barrier, 1, device_id={"fs": base + peer}, device_id_type=pl.DeviceIdType.MESH)
    pl.semaphore_signal(barrier, 1, device_id={"tp": 1 - c}, device_id_type=pl.DeviceIdType.MESH)

    for s in range(1, nz):
        pl.semaphore_signal(barrier, 1, device_id={"fs": lax.rem(z + s, nz) * GROUP + q},
                            device_id_type=pl.DeviceIdType.MESH)
    pl.semaphore_wait(barrier, 3 + nz)

    def piece(k, peer):
        if k == 2:
            return wd.at[at(peer * u, u), :]
        return (wg, wu)[k].at[:, at(peer * u, u)]

    def landing(k, owner):
        if k == 2:
            return od.at[:, at(owner * r, r)]
        return outs[k].at[at(owner * r, r), :]

    weights = []
    for k in range(3):
        for d, peer in enumerate((qa, qb, qd)):
            copy = remote(piece(k, peer), landing(k, f), w_s.at[k, d], w_r.at[k, d], fs=base + peer)
            copy.start()
            weights.append(copy)
    mine = at(c * half, half)
    near = []
    for i in range(3):
        for d, peer in enumerate((qa, qb)):
            copy = remote(xs[i].at[mine, :], ts[i].at[q, mine, :], n_s.at[i, d], n_r.at[i, d], fs=base + peer)
            copy.start()
            near.append(copy)
    local = []
    for k in range(3):
        copy = pltpu.make_async_copy(piece(k, q), landing(k, f), loc.at[k])
        copy.start()
        local.append(copy)
    for i in range(3):
        copy = pltpu.make_async_copy(xs[i], ts[i].at[q], loc.at[3 + i])
        copy.start()
        local.append(copy)

    def block(k, b):
        if k == 2:
            return od.at[:, at(b * GROUP * r, GROUP * r)]
        return outs[k].at[at(b * GROUP * r, GROUP * r), :]

    def right(k, s):
        b = block(k, z - s)
        return remote(b, b, r_s.at[s, k], r_r.at[s, k], fs=f + GROUP)

    def left(k, s):
        b = block(k, z + s)
        return remote(b, b, l_s.at[s, k], l_r.at[s, k], fs=f - GROUP)

    def arrived(k, s):
        @pl.when(z - s - 1 >= 0)
        def _():
            b = block(k, z - s - 1)
            remote(b, b, r_s.at[s, k], r_r.at[s, k], fs=f - GROUP).wait_recv()

        @pl.when(z + s + 1 < nz)
        def _():
            b = block(k, z + s + 1)
            remote(b, b, l_s.at[s, k], l_r.at[s, k], fs=f + GROUP).wait_recv()

    def onward(k, s, act):
        @pl.when(jnp.logical_and(z - s >= 0, last))
        def _():
            act(right(k, s))

        @pl.when(jnp.logical_and(z + s < nz, first))
        def _():
            act(left(k, s))

    begin, sent = (lambda copy: copy.start()), (lambda copy: copy.wait_send())

    row = lax.broadcasted_iota(jnp.int32, (rows, tile), 0)

    wide_tile = 2 * tile if d_model % (2 * tile) == 0 else tile

    def later(v, steps):
        return jnp.where(row >= steps, pltpu.roll(v, steps, 0), 0.0)

    def earlier(v, steps):
        return jnp.where(row < rows - steps, pltpu.roll(v, rows - steps, 0), 0.0)

    def forward(t, keep):
        @pl.loop(0, GROUP)
        def _(b):
            @pl.loop(0, u // tile)
            def _(j):
                cols, seq = at(j * tile, tile), at(b * rows, rows)
                x = t[b]
                gate = mm(x, og[:, cols]).astype(jnp.bfloat16).astype(jnp.float32)
                up = mm(x, ou[:, cols])
                conv = (bias[:, cols] + taps[2:3, cols] * gate + taps[1:2, cols] * later(gate, 1)
                        + taps[0:1, cols] * later(gate, 2))
                out = conv / (1.0 + jnp.exp(-conv)) * up
                if keep:
                    conv_s[seq, cols] = conv
                    up_s[seq, cols] = up
                    hid_t[at(j * tile, tile), seq] = out.T.astype(jnp.bfloat16)
                else:
                    hid[seq, cols] = out.astype(jnp.bfloat16)

    def down_grad():
        @pl.loop(0, d_model // wide_tile)
        def _(j):
            cols = at(j * wide_tile, wide_tile)
            cot = t2[:, :, cols].reshape(GROUP * rows, wide_tile)
            gp[:, cols] = mm(hid_t[...], cot).astype(jnp.bfloat16)

    def backward():
        @pl.loop(0, GROUP)
        def _(b):
            @pl.loop(0, u // tile)
            def _(j):
                cols, seq = at(j * tile, tile), at(b * rows, rows)
                dh = mm(t2[b], od[at(j * tile, tile), :], ((1,), (1,)))
                conv = conv_s[seq, cols]
                sig = 1.0 / (1.0 + jnp.exp(-conv))
                dup[seq, cols] = (dh * (conv * sig)).astype(jnp.bfloat16)
                dc = dh * up_s[seq, cols] * sig * (1.0 + conv * (1.0 - sig))
                dg = (taps[2:3, cols] * dc + taps[1:2, cols] * earlier(dc, 1)
                      + taps[0:1, cols] * earlier(dc, 2))
                dgate[seq, cols] = dg.astype(jnp.bfloat16)

    def late_out(owner):
        seq = at(owner * rows, rows)

        @pl.loop(0, d_model // wide_tile)
        def _(j):
            cols = at(j * wide_tile, wide_tile)
            yp[seq, cols] = mm(hid[seq, :], od[:, cols]).astype(jnp.bfloat16)

    def early_out(owner):
        seq = at(owner * rows, rows)

        @pl.loop(0, d_model // wide_tile)
        def _(j):
            cols = at(j * wide_tile, wide_tile)
            part = mm(dup[seq, :], ou[cols, :], ((1,), (1,))) + mm(dgate[seq, :], og[cols, :], ((1,), (1,)))
            xp[seq, cols] = part.astype(jnp.bfloat16)

    def enter(k):
        local[k].wait()
        for d in range(3):
            weights[3 * k + d].wait_recv()
        onward(k, 0, begin)

    enter(0)
    enter(1)
    partner = []

    def pass_on(i, owner, kind):
        there = ts[i].at[owner, mine, :]
        copy = remote(there, there, p_s.at[i, kind], p_r.at[i, kind], tp=1 - c)
        copy.start()
        partner.append((copy, i, owner, kind))

    far = []
    for i in range(3):
        near[2 * i].wait_recv()
        there = ts[i].at[qa, mine, :]
        copy = remote(there, there, n_s.at[i, 2], n_r.at[i, 2], fs=base + qb)
        copy.start()
        far.append(copy)
        pass_on(i, qa, 0)
        if i < 2 and nz > 2:
            arrived(i, 0)
            onward(i, 1, begin)
    for i in range(3):
        near[2 * i + 1].wait_recv()
        pass_on(i, qb, 1)
    for s in range(2, nz - 1):
        for k in range(2):
            arrived(k, s - 1)
            onward(k, s, begin)
    enter(2)
    for i in range(3):
        far[i].wait_recv()
        pass_on(i, qd, 2)
    if nz > 1:
        arrived(0, nz - 2)
        arrived(1, nz - 2)
    other = at((1 - c) * half, half)
    for copy, i, owner, kind in partner:
        there = ts[i].at[(qb, qa, qd)[kind], other, :]
        remote(there, there, p_s.at[i, kind], p_r.at[i, kind], tp=1 - c).wait_recv()
    for copy in local[3:]:
        copy.wait()

    jobs = [lambda: forward(t1, True), lambda: forward(t0, False), down_grad]
    for s in range(1, nz - 1):
        if jobs:
            jobs.pop(0)()
        arrived(2, s - 1)
        onward(2, s, begin)
    while jobs:
        jobs.pop(0)()
    grads = []
    for s in range(1, nz):
        to = lax.rem(z + s, nz)
        copy = remote(gp.at[:, at(to * wide, wide)], gin.at[s], z_s.at[s], z_r.at[s], fs=to * GROUP + q)
        copy.start()
        grads.append(copy)
    if nz > 1:
        arrived(2, nz - 2)

    parts, finals = (yp, xp), (y, dx)
    order = (qd, qa, qb, q)
    theirs = (qd, qb, qa, q)
    cores, sends = {}, {}

    def to_core(t, n):
        src = parts[t].at[at(theirs[n] * rows + (1 - c) * half, half), :]
        copy = remote(src, core.at[t, n], c_s.at[t, n], c_r.at[t, n], tp=1 - c)
        copy.start()
        cores[t, n] = copy

    def send(t, n, slot, peer):
        copy = remote(summed.at[t, n], got.at[t, slot], a_s.at[t, slot], a_r.at[t, slot], fs=base + peer)
        copy.start()
        sends[t, slot] = copy

    def join(t, n):
        cores[t, n].wait_recv()
        own = parts[t].at[at(order[n] * rows + c * half, half), :]
        total(summed.at[t, n], [own, core.at[t, n]], half)
        if n == 0:
            send(t, 0, 0, qa)
        if n == 1:
            send(t, 1, 1, qa)

    def onto_second(t):
        sends[t, 0].wait_recv()
        total(core.at[t, 0], [summed.at[t, 2], got.at[t, 0]], half)
        copy = remote(core.at[t, 0], got.at[t, 2], a_s.at[t, 2], a_r.at[t, 2], fs=base + qb)
        copy.start()
        sends[t, 2] = copy

    ends = []

    def finish(t):
        sends[t, 1].wait_recv()
        sends[t, 2].wait_recv()
        total(finals[t].at[mine, :], [summed.at[t, 3], got.at[t, 1], got.at[t, 2]], half)
        there = finals[t].at[mine, :]
        copy = remote(there, there, e_s.at[t], e_r.at[t], tp=1 - c)
        copy.start()
        ends.append(copy)

    def produce(t, make):
        make(qd)
        to_core(t, 0)
        make(qa)
        make(qb)
        to_core(t, 1)
        to_core(t, 2)
        join(t, 0)
        make(q)
        to_core(t, 3)
        for n in (1, 2):
            join(t, n)

    produce(0, late_out)
    backward()
    join(0, 3)
    onto_second(0)
    produce(1, early_out)
    join(1, 3)
    finish(0)
    onto_second(1)
    for copy in grads:
        copy.wait_recv()
    total(gsum, [gp.at[:, at(z * wide, wide)]] + [gin.at[s] for s in range(1, nz)], u)
    handed = []
    for d, peer in enumerate((qa, qb, qd)):
        copy = remote(gsum.at[:, at(peer * r, r)], g.at[at(q * u, u), :], g_s.at[d], g_r.at[d], fs=base + peer)
        copy.start()
        handed.append(copy)
    g[at(q * u, u), :] = gsum[:, at(q * r, r)]
    finish(1)
    for copy in handed + ends:
        copy.wait_recv()
    for copy in weights + near + far + [p[0] for p in partner]:
        copy.wait_send()
    for copy in list(cores.values()) + grads + handed + ends + list(sends.values()):
        copy.wait_send()
    for s in range(nz - 1):
        for k in range(3):
            onward(k, s, sent)


def layer(nz, xs, w_gate, w_up, w_down, taps, bias):
    rows, d = xs[0].shape
    u = w_gate.shape[1] // GROUP
    r = w_gate.shape[0]
    half, toks = rows // 2, GROUP * rows
    tile = 256 if u % 256 == 0 else 128
    sems = lambda *shape: [pltpu.SemaphoreType.DMA(shape)] * 2
    b16, f32 = jnp.bfloat16, jnp.float32
    out = jax.ShapeDtypeStruct((rows, d), b16)
    hops = max(nz - 1, 1)
    return pl.pallas_call(
        functools.partial(layer_kernel, nz, tile),
        out_shape=(out, out, jax.ShapeDtypeStruct((u * GROUP, r), b16)),
        in_specs=[VMEM] * 8,
        out_specs=(VMEM,) * 3,
        scratch_shapes=[pltpu.VMEM((GROUP, rows, d), b16)] * 3
        + [pltpu.VMEM((d, u), b16)] * 2
        + [pltpu.VMEM((u, d), b16), pltpu.VMEM((toks, u), b16), pltpu.VMEM((u, toks), b16),
           pltpu.VMEM((toks, u), f32), pltpu.VMEM((toks, u), f32),
           pltpu.VMEM((toks, u), b16), pltpu.VMEM((toks, u), b16),
           pltpu.VMEM((toks, d), b16), pltpu.VMEM((toks, d), b16), pltpu.VMEM((u, d), b16),
           pltpu.VMEM((2, 4, half, d), b16), pltpu.VMEM((2, 4, half, d), b16), pltpu.VMEM((2, 3, half, d), b16),
           pltpu.VMEM((nz, u, GROUP * r), b16), pltpu.VMEM((u, GROUP * r), b16),
           pltpu.SemaphoreType.DMA((6,))]
        + sems(3, 3) + sems(3, 3) + sems(3, 3) + sems(hops, 3) + sems(hops, 3)
        + sems(2, 4) + sems(2, 3) + sems(nz) + sems(3) + sems(2),
        compiler_params=pltpu.CompilerParams(collective_id=0, has_side_effects=True, vmem_limit_bytes=VMEM_BYTES),
        name="layer_group",
    )(*xs, w_gate, w_up, w_down, taps, bias)


def shift_later(field, steps):
    pad = jnp.zeros((steps, field.shape[1]), jnp.float32)
    return jnp.concatenate([pad, field[: field.shape[0] - steps]], axis=0)


def shift_earlier(field, steps):
    pad = jnp.zeros((steps, field.shape[1]), jnp.float32)
    return jnp.concatenate([field[steps:], pad], axis=0)


def contract_last(left, right):
    return lax.dot_general(
        left, right, (((1,), (1,)), ((), ())), preferred_element_type=jnp.float32
    )


def hidden_parts(inputs, gate_full, up_full, taps, bias):
    gate = (
        jnp.dot(inputs, gate_full, preferred_element_type=jnp.float32)
        .astype(jnp.bfloat16)
        .astype(jnp.float32)
    )
    up = jnp.dot(inputs, up_full, preferred_element_type=jnp.float32)
    conv = bias + taps[2] * gate + taps[1] * shift_later(gate, 1) + taps[0] * shift_later(gate, 2)
    act = jax.nn.silu(conv)
    hidden = (act * up).astype(jnp.bfloat16)
    return (conv, act, up, hidden)


def forward_pass(x_late, gate_full, up_full, down_full, taps, bias):
    conv, act, up, hidden = hidden_parts(x_late, gate_full, up_full, taps, bias)
    partial_value = jnp.dot(hidden, down_full, preferred_element_type=jnp.float32)
    return lax.psum(partial_value.astype(jnp.bfloat16), "tp")


def backward_pass(x_early, cotangent, gate_full, up_full, down_full, taps, bias, grad_down):
    conv, act, up, hidden = hidden_parts(x_early, gate_full, up_full, taps, bias)
    dhidden = contract_last(cotangent, down_full)
    summed = lax.psum_scatter(
        lax.dot_general(
            cotangent, hidden, (((0,), (0,)), ((), ())), preferred_element_type=jnp.float32
        ),
        "fs",
        scatter_dimension=0,
        tiled=True,
    )
    grad_down_out = grad_down + summed.T
    dup = (dhidden * act).astype(jnp.bfloat16)
    sig = jax.nn.sigmoid(conv)
    dconv = dhidden * up * sig * (1.0 + conv * (1.0 - sig))
    dgate = taps[2] * dconv + taps[1] * shift_earlier(dconv, 1) + taps[0] * shift_earlier(dconv, 2)
    dgate = dgate.astype(jnp.bfloat16)
    partial_value = contract_last(dup, up_full) + contract_last(dgate, gate_full)
    dx_early = lax.psum(partial_value.astype(jnp.bfloat16), "tp")
    return (dx_early, grad_down_out)


def shards(x_late, x_early, cotangent, w_gate, w_up, w_down, conv_taps, conv_bias, grad_down):
    width = w_gate.shape[1]
    offset = lax.axis_index("tp") * width
    taps = lax.dynamic_slice_in_dim(conv_taps, offset, width, 1)
    bias = lax.dynamic_slice_in_dim(conv_bias, offset, width, 0)
    gate_full, up_full = (
        lax.all_gather(w_gate, "fs", axis=0, tiled=True),
        lax.all_gather(w_up, "fs", axis=0, tiled=True),
    )
    down_full = lax.all_gather(w_down, "fs", axis=1, tiled=True)
    y_late = forward_pass(x_late, gate_full, up_full, down_full, taps, bias)
    dx_early, grad_down_out = backward_pass(
        x_early, cotangent, gate_full, up_full, down_full, taps, bias, grad_down
    )
    return (y_late, dx_early, grad_down_out)


def grouped_shards(nz, x_late, x_early, cotangent, w_gate, w_up, w_down, conv_taps, conv_bias, grad_down):
    units = w_gate.shape[1] // GROUP
    start = (lax.axis_index("tp") * GROUP + lax.rem(lax.axis_index("fs"), GROUP)) * units
    taps = lax.dynamic_slice_in_dim(conv_taps, start, units, 1)
    bias = lax.dynamic_slice_in_dim(conv_bias, start, units, 0)
    y_late, dx_early, grad = layer(
        nz, (x_late, x_early, cotangent), w_gate, w_up, w_down, taps, bias.reshape(1, units)
    )
    return (y_late, dx_early, grad_down + grad.astype(jnp.float32))


def solution(mesh):
    def step(*arrays):
        x_late, w_gate = arrays[0], arrays[3]
        fs, tp = mesh.shape["fs"], mesh.shape["tp"]
        units, rest = divmod(w_gate.shape[1], GROUP)
        lanes_ok = rest == 0 and units % 128 == 0 and w_gate.shape[0] % 128 == 0
        if tp == 2 and fs % GROUP == 0 and lanes_ok and x_late.shape[0] % 32 == 0:
            return grouped_shards(fs // GROUP, *arrays)
        return shards(*arrays)

    placed = (
        P("fs", None),
        P("fs", None),
        P("fs", None),
        P("fs", "tp"),
        P("fs", "tp"),
        P("tp", "fs"),
        P(),
        P(),
        P("tp", "fs"),
    )
    return jax.shard_map(
        step,
        mesh=mesh,
        in_specs=placed,
        out_specs=(P("fs", None), P("fs", None), P("tp", "fs")),
        check_vma=False,
    )
```

profile of v0, /device:TPU:0, one launch (start us, length us, event | category | flops | bytes accessed | tf_op | source)
XLA Modules:
  0.0 197.9 jit_solution(14732989446540928877)
XLA Ops:
  0.6 0.0 copy-start
  0.7 1.4 dynamic_slice.7
  2.0 0.0 copy-done
  2.0 0.6 constant_dynamic-slice_fusion.taps
  2.6 0.0 copy-start.1
  2.6 190.5 %layer_group.1 = (bf16[256,2048]{1,0:T(8,128)(2,1)}, bf16[256,2048]{1,0:T(8,128)(2,1)}, bf16[2048,128]{1,0:T(8,128)(2,1)}) custom-call(bf16[256,2048]{1,0:T(8,128)(2,1)} %x0.1, bf16[256,2048]{1,0:T(8,128)(2,1)} %x1.1, bf16[256,2048]{1,0:T(8,128)(2,1)} %x2.1, bf16[128,2048]{1,0:T(8,128)(2,1)} %wg.1, bf16[128,2048]{1,0:T(8,128)(2,1)} %wu.1, ...), custom_call_target="tpu_custom_call" | custom-call | tf_op jit(solution)/shard_map/layer_group/pallas_call | solution.py:369
  193.1 0.0 copy-done.1
  193.1 0.0 copy-start.3
  193.1 2.2 %convert_add_fusion = f32[2048,128]{1,0:T(8,128)} fusion(f32[2048,128]{1,0:T(8,128)S(1)} %copy-done.1, bf16[2048,128]{1,0:T(8,128)(2,1)} %get-tuple-element.8), kind=kLoop, calls=%fused_computation | loop fusion | flops 524288 | bytes 2621440 | tf_op jit(solution)/shard_map/add | solution.py:472
  195.3 0.0 copy-done.3
  195.3 0.0 copy-start.2
  195.3 1.0 copy.14
  196.3 0.6 copy-done.2
  196.9 1.0 copy.15
Async XLA Ops:
  0.6 1.4 copy-start
  2.6 190.5 %copy-start.1 = (f32[2048,128]{1,0:T(8,128)S(1)}, f32[2048,128]{1,0:T(8,128)}, u32[]{:S(2)}) copy-start(f32[2048,128]{1,0:T(8,128)} %param.17) | copy-start | bytes 3145732
  193.1 2.2 %copy-start.3 = (bf16[256,2048]{1,0:T(8,128)(2,1)S(1)}, bf16[256,2048]{1,0:T(8,128)(2,1)}, u32[]{:S(2)}) copy-start(bf16[256,2048]{1,0:T(8,128)(2,1)} %get-tuple-element.12) | copy-start | bytes 3145732
  195.3 1.6 copy-start.2
where the time goes:
time: 198 us
  Pallas kernels  190 us (96%)
  local copies, waits for them, and re-layouts  4.56 us (2%)
  other arithmetic  2.19 us (1%)
    pallas_call x1, Pallas kernels, layer(): pl.pallas_call(functools.partial(layer_kernel, nz, tile), out_shape=(out,...  190 us

commit v1 on v0

v1 whole, which is shorter than its diff:
```python
import functools

import jax
import jax.numpy as jnp
from jax import lax
from jax.experimental import pallas as pl
from jax.experimental.pallas import tpu as pltpu
from jax.sharding import PartitionSpec as P

GROUP = 4
VMEM_BYTES = 63 * 1024 * 1024
VMEM = pl.BlockSpec(memory_space=pltpu.VMEM)


def place():
    f, c = lax.axis_index("fs"), lax.axis_index("tp")
    q, z = lax.rem(f, GROUP), lax.div(f, GROUP)
    qx = q + 1 - 2 * lax.rem(q, 2)
    qy = q + 2 - 4 * lax.div(q, 2)
    qa, qb = qx + c * (qy - qx), qy + c * (qx - qy)
    return f, c, q, z, qa, qb, GROUP - 1 - q


def at(start, size):
    return pl.ds(pl.multiple_of(start, size), size)


def remote(src, dst, send, recv, **device):
    return pltpu.make_async_remote_copy(
        src_ref=src, dst_ref=dst, send_sem=send, recv_sem=recv,
        device_id=device, device_id_type=pl.DeviceIdType.MESH,
    )


def total(dst, srcs, rows, step=32):
    @pl.loop(0, rows, step=step)
    def _(i):
        sl = pl.ds(pl.multiple_of(i, step), step)
        out = srcs[0][sl, :].astype(jnp.float32)
        for s in srcs[1:]:
            out = out + s[sl, :].astype(jnp.float32)
        dst[sl, :] = out.astype(dst.dtype)


def mm(left, right, dims=((1,), (0,))):
    return lax.dot_general(left, right, (dims, ((), ())), preferred_element_type=jnp.float32)


def layer_kernel(nz, tile, x0, x1, x2, wg, wu, wd, taps, bias, gd, y, dx, g,
                 t0, t1, t2, og, ou, od, hid, hid_t, conv_s, up_s, dup, dgate, yp, xp, gp,
                 core, summed, got, gin_r, gin_l, gsum, hand,
                 loc, w_s, w_r, n_s, n_r, p_s, p_r, r_s, r_r, l_s, l_r,
                 c_s, c_r, a_s, a_r, zr_s, zr_r, zl_s, zl_r, g_s, g_r, e_s, e_r):
    f, c, q, z, qa, qb, qd = place()
    base = z * GROUP
    xs, ts, outs = (x0, x1, x2), (t0, t1, t2), (og, ou, od)
    rows, d_model = x0.shape
    half = rows // 2
    r, u = wg.shape[0], og.shape[1]
    wide = GROUP * r
    first, last = z > 0, z < nz - 1
    low, high = z == 0, z == nz - 1
    units = (c * GROUP + q) * u

    barrier = pltpu.get_barrier_semaphore()
    for peer in (qa, qb, qd):
        pl.semaphore_signal(barrier, 1, device_id={"fs": base + peer}, device_id_type=pl.DeviceIdType.MESH)
    pl.semaphore_signal(barrier, 1, device_id={"tp": 1 - c}, device_id_type=pl.DeviceIdType.MESH)
    for s in range(1, nz):
        pl.semaphore_signal(barrier, 1, device_id={"fs": lax.rem(z + s, nz) * GROUP + q},
                            device_id_type=pl.DeviceIdType.MESH)
    pl.semaphore_wait(barrier, 3 + nz)

    def piece(k, peer):
        if k == 2:
            return wd.at[at(peer * u, u), :]
        return (wg, wu)[k].at[:, at(peer * u, u)]

    def landing(k, owner):
        if k == 2:
            return od.at[:, at(owner * r, r)]
        return outs[k].at[at(owner * r, r), :]

    def block(k, b):
        if k == 2:
            return od.at[:, at(b * wide, wide)]
        return outs[k].at[at(b * wide, wide), :]

    def right(k, s):
        b = block(k, z - s)
        return remote(b, b, r_s.at[s, k], r_r.at[s, k], fs=f + GROUP)

    def left(k, s):
        b = block(k, z + s)
        return remote(b, b, l_s.at[s, k], l_r.at[s, k], fs=f - GROUP)

    def from_left(k, s):
        b = block(k, z - s - 1)
        return remote(b, b, r_s.at[s, k], r_r.at[s, k], fs=f - GROUP)

    def from_right(k, s):
        b = block(k, z + s + 1)
        return remote(b, b, l_s.at[s, k], l_r.at[s, k], fs=f + GROUP)

    def onward(k, s, act):
        @pl.when(jnp.logical_and(z - s >= 0, last))
        def _():
            act(right(k, s))

        @pl.when(jnp.logical_and(z + s < nz, first))
        def _():
            act(left(k, s))

    begin, sent = (lambda copy: copy.start()), (lambda copy: copy.wait_send())

    def along(k, src, owner):
        there = landing(k, owner)

        @pl.when(last)
        def _():
            remote(src, there, r_s.at[0, k], r_r.at[0, k], fs=f + GROUP).start()

        @pl.when(first)
        def _():
            remote(src, there, l_s.at[0, k], l_r.at[0, k], fs=f - GROUP).start()

    def relay(k, s):
        @pl.when(jnp.logical_and(z - s - 1 >= 0, last))
        def _():
            from_left(k, s).wait_recv()
            right(k, s + 1).start()

        @pl.when(jnp.logical_and(z + s + 1 < nz, first))
        def _():
            from_right(k, s).wait_recv()
            left(k, s + 1).start()

    def ended(k, s):
        @pl.when(high)
        def _():
            from_left(k, s).wait_recv()

        @pl.when(low)
        def _():
            from_right(k, s).wait_recv()

    mine, other = at(c * half, half), at((1 - c) * half, half)
    weights, near, local = {}, {}, []

    def spread(k):
        for d, peer in enumerate((qa, qb, qd)):
            copy = remote(piece(k, peer), landing(k, f), w_s.at[k, d], w_r.at[k, d], fs=base + peer)
            copy.start()
            weights[k, d] = copy

    def share(i):
        for d, peer in enumerate((qa, qb)):
            copy = remote(xs[i].at[mine, :], ts[i].at[q, mine, :], n_s.at[i, d], n_r.at[i, d], fs=base + peer)
            copy.start()
            near[i, d] = copy

    along(0, piece(0, q), f)
    spread(0)
    along(1, piece(1, q), f)
    spread(1)
    share(1)
    share(0)
    spread(2)
    share(2)
    for k in range(3):
        copy = pltpu.make_async_copy(piece(k, q), landing(k, f), loc.at[k])
        copy.start()
        local.append(copy)
    for i in range(3):
        copy = pltpu.make_async_copy(xs[i], ts[i].at[q], loc.at[3 + i])
        copy.start()
        local.append(copy)

    row = lax.broadcasted_iota(jnp.int32, (rows, tile), 0)

    def later(v, steps):
        return jnp.where(row >= steps, pltpu.roll(v, steps, 0), 0.0)

    def earlier(v, steps):
        return jnp.where(row < rows - steps, pltpu.roll(v, rows - steps, 0), 0.0)

    def forward(t, keep):
        @pl.loop(0, GROUP)
        def _(b):
            @pl.loop(0, u // tile)
            def _(j):
                cols, seq, par = at(j * tile, tile), at(b * rows, rows), at(units + j * tile, tile)
                x = t[b]
                gate = mm(x, og[:, cols]).astype(jnp.bfloat16).astype(jnp.float32)
                up = mm(x, ou[:, cols])
                conv = (bias[:, par] + taps[2:3, par] * gate + taps[1:2, par] * later(gate, 1)
                        + taps[0:1, par] * later(gate, 2))
                out = conv / (1.0 + jnp.exp(-conv)) * up
                if keep:
                    conv_s[seq, cols] = conv
                    up_s[seq, cols] = up
                    hid_t[at(j * tile, tile), seq] = out.T.astype(jnp.bfloat16)
                else:
                    hid[seq, cols] = out.astype(jnp.bfloat16)

    upper = lax.div(2 * z, nz)

    def down_grad():
        for i in range(nz):
            o = nz - 1 - i + upper * (2 * i - (nz - 1))
            cols = at(o * wide, wide)
            cot = t2[:, :, cols].reshape(GROUP * rows, wide)
            gp[:, cols] = mm(hid_t[...], cot).astype(jnp.bfloat16)
            if i < nz - 1:
                @pl.when(low)
                def _():
                    remote(gp.at[:, cols], gin_r.at[i], zr_s.at[i], zr_r.at[i], fs=f + GROUP).start()

                @pl.when(high)
                def _():
                    remote(gp.at[:, cols], gin_l.at[i], zl_s.at[i], zl_r.at[i], fs=f - GROUP).start()

    def gone(i):
        cols = at((nz - 1 - i) * wide, wide)
        return remote(gp.at[:, cols], gin_r.at[i], zr_s.at[i], zr_r.at[i], fs=f + GROUP)

    def chain(j):
        o = nz - 2 + z - j
        got_r = remote(gin_r.at[j], gin_r.at[j], zr_s.at[j], zr_r.at[j], fs=f - GROUP)
        got_l = remote(gin_l.at[j], gin_l.at[j], zl_s.at[j], zl_r.at[j], fs=f + GROUP)

        @pl.when(jnp.logical_and(first, o <= nz - 1))
        def _():
            got_r.wait_recv()

        if j < nz - 2:
            @pl.when(jnp.logical_and(first, o <= nz - 1))
            def _():
                cols = at(o * wide, wide)
                total(gp.at[:, cols], [gp.at[:, cols], gin_r.at[j]], u)
                remote(gp.at[:, cols], gin_r.at[j + 1], zr_s.at[j + 1], zr_r.at[j + 1], fs=f + GROUP).start()

        p = z + 1 - nz + 1 + j

        @pl.when(jnp.logical_and(last, p >= 0))
        def _():
            got_l.wait_recv()

        if j < nz - 2:
            @pl.when(jnp.logical_and(last, p >= 0))
            def _():
                cols = at(p * wide, wide)
                total(gp.at[:, cols], [gp.at[:, cols], gin_l.at[j]], u)
                remote(gp.at[:, cols], gin_l.at[j + 1], zl_s.at[j + 1], zl_r.at[j + 1], fs=f - GROUP).start()

    def backward():
        @pl.loop(0, GROUP)
        def _(b):
            @pl.loop(0, u // tile)
            def _(j):
                cols, seq, par = at(j * tile, tile), at(b * rows, rows), at(units + j * tile, tile)
                dh = mm(t2[b], od[at(j * tile, tile), :], ((1,), (1,)))
                conv = conv_s[seq, cols]
                sig = 1.0 / (1.0 + jnp.exp(-conv))
                dup[seq, cols] = (dh * (conv * sig)).astype(jnp.bfloat16)
                dc = dh * up_s[seq, cols] * sig * (1.0 + conv * (1.0 - sig))
                dg = (taps[2:3, par] * dc + taps[1:2, par] * earlier(dc, 1)
                      + taps[0:1, par] * earlier(dc, 2))
                dgate[seq, cols] = dg.astype(jnp.bfloat16)

    mirrored = z + upper * (nz - 1 - 2 * z)

    def turn(i):
        near_side = lax.div(mirrored - i + nz, nz)
        v = i + near_side * (mirrored - 2 * i)
        return v + upper * (nz - 1 - 2 * v)

    sub = 256 if wide % 256 == 0 else 128

    def late_block(i):
        start = turn(i) * wide

        @pl.loop(0, wide // sub)
        def _(j):
            cols = at(start + j * sub, sub)
            yp[:, cols] = mm(hid[...], od[:, cols]).astype(jnp.bfloat16)

    def early_block(i):
        @pl.loop(0, wide // sub)
        def _(j):
            cols = at(i * wide + j * sub, sub)
            part = mm(dup[...], ou[cols, :], ((1,), (1,))) + mm(dgate[...], og[cols, :], ((1,), (1,)))
            xp[:, cols] = part.astype(jnp.bfloat16)

    parts, finals = (yp, xp), (y, dx)
    order = (qd, qa, qb, q)
    theirs = (qd, qb, qa, q)
    cores, sends, ends = {}, {}, []

    def span(t, i):
        return at(turn(i) * wide, wide) if t == 0 else at(i * wide, wide)

    def to_core(t, i):
        cols = span(t, i)
        for n in range(4):
            src = parts[t].at[at(theirs[n] * rows + (1 - c) * half, half), cols]
            copy = remote(src, core.at[t, n, :, cols], c_s.at[t, i, n], c_r.at[t, i, n], tp=1 - c)
            copy.start()
            cores[t, i, n] = copy

    def send(t, i, src, slot, peer):
        cols = span(t, i)
        copy = remote(src, got.at[t, slot, :, cols], a_s.at[t, i, slot], a_r.at[t, i, slot], fs=base + peer)
        copy.start()
        sends[t, i, slot] = copy

    def join(t, i):
        cols = span(t, i)
        for n in range(4):
            cores[t, i, n].wait_recv()
            own = parts[t].at[at(order[n] * rows + c * half, half), cols]
            total(summed.at[t, n, :, cols], [own, core.at[t, n, :, cols]], half)
            if n < 2:
                send(t, i, summed.at[t, n, :, cols], n, qa)

    def second(t, i):
        cols = span(t, i)
        sends[t, i, 0].wait_recv()
        total(core.at[t, 0, :, cols], [summed.at[t, 2, :, cols], got.at[t, 0, :, cols]], half)
        send(t, i, core.at[t, 0, :, cols], 2, qb)

    def finish(t, i):
        cols = span(t, i)
        sends[t, i, 1].wait_recv()
        sends[t, i, 2].wait_recv()
        there = finals[t].at[mine, cols]
        total(there, [summed.at[t, 3, :, cols], got.at[t, 1, :, cols], got.at[t, 2, :, cols]], half)
        copy = remote(there, there, e_s.at[t, i], e_r.at[t, i], tp=1 - c)
        copy.start()
        ends.append(copy)

    stages = (to_core, join, second, finish)

    def step(t, i, *which):
        for s in which:
            if 0 <= i - s < nz:
                stages[s](t, i - s)

    partner, far = [], {}

    def pass_on(i, owner, kind):
        there = ts[i].at[owner, mine, :]
        copy = remote(there, there, p_s.at[i, kind], p_r.at[i, kind], tp=1 - c)
        copy.start()
        partner.append(copy)

    def adjacent(i):
        near[i, 0].wait_recv()
        there = ts[i].at[qa, mine, :]
        copy = remote(there, there, n_s.at[i, 2], n_r.at[i, 2], fs=base + qb)
        copy.start()
        far[i] = copy
        pass_on(i, qa, 0)
        near[i, 1].wait_recv()
        pass_on(i, qb, 1)

    def opposite(i):
        far[i].wait_recv()
        pass_on(i, qd, 2)

    def complete(i):
        for kind, owner in enumerate((qb, qa, qd)):
            there = ts[i].at[owner, other, :]
            remote(there, there, p_s.at[i, kind], p_r.at[i, kind], tp=1 - c).wait_recv()
        local[3 + i].wait()

    for k in range(2):
        for d, peer in enumerate((qa, qb, qd)):
            weights[k, d].wait_recv()
            along(k, landing(k, base + peer), base + peer)
        local[k].wait()
    adjacent(1)
    if nz > 2:
        relay(0, 0)
        relay(1, 0)
    adjacent(0)
    for d in range(3):
        weights[2, d].wait_recv()
    local[2].wait()
    for s in range(1, nz - 2):
        relay(0, s)
        relay(1, s)
    onward(2, 0, begin)
    adjacent(2)
    opposite(1)
    opposite(0)
    complete(1)
    for s in range(nz - 1):
        ended(0, s)
        ended(1, s)
    forward(t1, True)
    if nz > 2:
        relay(2, 0)
    opposite(2)
    complete(2)
    down_grad()
    complete(0)
    forward(t0, False)
    for s in range(1, nz - 2):
        relay(2, s)

    for i in range(nz):
        if i == nz - 1 and nz > 2:
            chain(0)
        if i > 0:
            ended(2, i - 1)
        late_block(i)
        step(0, i, 0, 1, 2)
    backward()
    step(0, nz, 1, 2)
    early_block(0)
    step(1, 0, 0)
    step(0, nz + 1, 2)
    for i in range(1, nz):
        early_block(i)
        step(1, i, 0, 1)
    for j in range(1, nz - 2):
        chain(j)
    for i in range(nz):
        finish(0, i)
    step(1, nz, 1)
    for i in range(nz):
        second(1, i)
        if i == min(1, nz - 1):
            if nz > 1:
                chain(nz - 2)
            home = gp.at[:, at(z * wide, wide)]
            if nz == 1:
                total(gsum, [home], u)
            else:
                lo_in, hi_in = gin_r.at[nz - 2], gin_l.at[nz - 2]
                for cond, srcs in ((low, [home, hi_in]), (high, [home, lo_in]),
                                   (jnp.logical_and(first, last), [home, lo_in, hi_in])):
                    @pl.when(cond)
                    def _(srcs=srcs):
                        total(gsum, srcs, u)
            handed = []
            for d, peer in enumerate((qa, qb, qd)):
                copy = remote(gsum.at[:, at(peer * r, r)], hand.at[at(q * u, u), :], g_s.at[d], g_r.at[d],
                              fs=base + peer)
                copy.start()
                handed.append(copy)
            hand[at(q * u, u), :] = gsum[:, at(q * r, r)]
        if i > 0:
            finish(1, i - 1)
    finish(1, nz - 1)
    for copy in handed:
        copy.wait_recv()

    @pl.loop(0, GROUP * u, step=128)
    def _(i):
        sl = at(i, 128)
        g[sl, :] = gd[sl, :] + hand[sl, :].astype(jnp.float32)

    for copy in ends:
        copy.wait_recv()
    for copies in (weights, near, far, cores, sends):
        for copy in copies.values():
            copy.wait_send()
    for copy in partner + handed + ends:
        copy.wait_send()
    for s in range(nz - 1):
        for k in range(3):
            onward(k, s, sent)
    for m in range(nz - 1):
        chunk = gp.at[:, at(0, wide)]

        @pl.when(jnp.logical_and(last, z <= m))
        def _():
            remote(chunk, gin_r.at[m], zr_s.at[m], zr_r.at[m], fs=f + GROUP).wait_send()

        @pl.when(jnp.logical_and(first, nz - 1 - z <= m))
        def _():
            remote(chunk, gin_l.at[m], zl_s.at[m], zl_r.at[m], fs=f - GROUP).wait_send()


def layer(nz, xs, w_gate, w_up, w_down, taps, bias, grad_down):
    rows, d = xs[0].shape
    u = w_gate.shape[1] // GROUP
    r = w_gate.shape[0]
    half, toks, wide = rows // 2, GROUP * rows, GROUP * r
    tile = 256 if u % 256 == 0 else 128
    sems = lambda *shape: [pltpu.SemaphoreType.DMA(shape)] * 2
    b16, f32 = jnp.bfloat16, jnp.float32
    out = jax.ShapeDtypeStruct((rows, d), b16)
    hops = max(nz - 1, 1)
    return pl.pallas_call(
        functools.partial(layer_kernel, nz, tile),
        out_shape=(out, out, jax.ShapeDtypeStruct((u * GROUP, r), f32)),
        in_specs=[VMEM] * 9,
        out_specs=(VMEM,) * 3,
        scratch_shapes=[pltpu.VMEM((GROUP, rows, d), b16)] * 3
        + [pltpu.VMEM((d, u), b16)] * 2
        + [pltpu.VMEM((u, d), b16), pltpu.VMEM((toks, u), b16), pltpu.VMEM((u, toks), b16),
           pltpu.VMEM((toks, u), f32), pltpu.VMEM((toks, u), f32),
           pltpu.VMEM((toks, u), b16), pltpu.VMEM((toks, u), b16),
           pltpu.VMEM((toks, d), b16), pltpu.VMEM((toks, d), b16), pltpu.VMEM((u, d), b16),
           pltpu.VMEM((2, 4, half, d), b16), pltpu.VMEM((2, 4, half, d), b16), pltpu.VMEM((2, 3, half, d), b16),
           pltpu.VMEM((hops, u, wide), b16), pltpu.VMEM((hops, u, wide), b16),
           pltpu.VMEM((u, wide), b16), pltpu.VMEM((u * GROUP, r), b16),
           pltpu.SemaphoreType.DMA((6,))]
        + sems(3, 3) + sems(3, 3) + sems(3, 3) + sems(hops, 3) + sems(hops, 3)
        + sems(2, nz, 4) + sems(2, nz, 3) + sems(hops) + sems(hops) + sems(3) + sems(2, nz),
        compiler_params=pltpu.CompilerParams(collective_id=0, has_side_effects=True, vmem_limit_bytes=VMEM_BYTES),
        name="layer_group",
    )(*xs, w_gate, w_up, w_down, taps, bias, grad_down)


def shift_later(field, steps):
    pad = jnp.zeros((steps, field.shape[1]), jnp.float32)
    return jnp.concatenate([pad, field[: field.shape[0] - steps]], axis=0)


def shift_earlier(field, steps):
    pad = jnp.zeros((steps, field.shape[1]), jnp.float32)
    return jnp.concatenate([field[steps:], pad], axis=0)


def contract_last(left, right):
    return lax.dot_general(
        left, right, (((1,), (1,)), ((), ())), preferred_element_type=jnp.float32
    )


def hidden_parts(inputs, gate_full, up_full, taps, bias):
    gate = (
        jnp.dot(inputs, gate_full, preferred_element_type=jnp.float32)
        .astype(jnp.bfloat16)
        .astype(jnp.float32)
    )
    up = jnp.dot(inputs, up_full, preferred_element_type=jnp.float32)
    conv = bias + taps[2] * gate + taps[1] * shift_later(gate, 1) + taps[0] * shift_later(gate, 2)
    act = jax.nn.silu(conv)
    hidden = (act * up).astype(jnp.bfloat16)
    return (conv, act, up, hidden)


def forward_pass(x_late, gate_full, up_full, down_full, taps, bias):
    conv, act, up, hidden = hidden_parts(x_late, gate_full, up_full, taps, bias)
    partial_value = jnp.dot(hidden, down_full, preferred_element_type=jnp.float32)
    return lax.psum(partial_value.astype(jnp.bfloat16), "tp")


def backward_pass(x_early, cotangent, gate_full, up_full, down_full, taps, bias, grad_down):
    conv, act, up, hidden = hidden_parts(x_early, gate_full, up_full, taps, bias)
    dhidden = contract_last(cotangent, down_full)
    summed = lax.psum_scatter(
        lax.dot_general(
            cotangent, hidden, (((0,), (0,)), ((), ())), preferred_element_type=jnp.float32
        ),
        "fs",
        scatter_dimension=0,
        tiled=True,
    )
    grad_down_out = grad_down + summed.T
    dup = (dhidden * act).astype(jnp.bfloat16)
    sig = jax.nn.sigmoid(conv)
    dconv = dhidden * up * sig * (1.0 + conv * (1.0 - sig))
    dgate = taps[2] * dconv + taps[1] * shift_earlier(dconv, 1) + taps[0] * shift_earlier(dconv, 2)
    dgate = dgate.astype(jnp.bfloat16)
    partial_value = contract_last(dup, up_full) + contract_last(dgate, gate_full)
    dx_early = lax.psum(partial_value.astype(jnp.bfloat16), "tp")
    return (dx_early, grad_down_out)


def shards(x_late, x_early, cotangent, w_gate, w_up, w_down, conv_taps, conv_bias, grad_down):
    width = w_gate.shape[1]
    offset = lax.axis_index("tp") * width
    taps = lax.dynamic_slice_in_dim(conv_taps, offset, width, 1)
    bias = lax.dynamic_slice_in_dim(conv_bias, offset, width, 0)
    gate_full, up_full = (
        lax.all_gather(w_gate, "fs", axis=0, tiled=True),
        lax.all_gather(w_up, "fs", axis=0, tiled=True),
    )
    down_full = lax.all_gather(w_down, "fs", axis=1, tiled=True)
    y_late = forward_pass(x_late, gate_full, up_full, down_full, taps, bias)
    dx_early, grad_down_out = backward_pass(
        x_early, cotangent, gate_full, up_full, down_full, taps, bias, grad_down
    )
    return (y_late, dx_early, grad_down_out)


def grouped_shards(nz, x_late, x_early, cotangent, w_gate, w_up, w_down, conv_taps, conv_bias, grad_down):
    return layer(
        nz, (x_late, x_early, cotangent), w_gate, w_up, w_down, conv_taps,
        conv_bias.reshape(1, conv_bias.shape[0]), grad_down,
    )


def solution(mesh):
    def step(*arrays):
        x_late, w_gate = arrays[0], arrays[3]
        fs, tp = mesh.shape["fs"], mesh.shape["tp"]
        units, rest = divmod(w_gate.shape[1], GROUP)
        lanes_ok = rest == 0 and units % 128 == 0 and w_gate.shape[0] % 128 == 0
        if tp == 2 and fs % GROUP == 0 and lanes_ok and x_late.shape[0] % 32 == 0:
            return grouped_shards(fs // GROUP, *arrays)
        return shards(*arrays)

    placed = (
        P("fs", None),
        P("fs", None),
        P("fs", None),
        P("fs", "tp"),
        P("fs", "tp"),
        P("tp", "fs"),
        P(),
        P(),
        P("tp", "fs"),
    )
    return jax.shard_map(
        step,
        mesh=mesh,
        in_specs=placed,
        out_specs=(P("fs", None), P("fs", None), P("tp", "fs")),
        check_vma=False,
    )
```

time: 198 us -> 160 us (0.81)
  Pallas kernels: 190 us -> 154 us
  other arithmetic: 2.19 us -> 0 us
    pallas_call x1, Pallas kernels: 190 us -> 154 us  [layer(): pl.pallas_call(functools.partial(layer_kernel, nz, tile), out_shape=(out,...]
    unnamed x10 -> x7, local copies, waits for them, and re-layouts: 2.59 us -> 4.97 us
    add x1 -> x0, other arithmetic: 2.19 us -> none  [grouped_shards(): return (y_late, dx_early, grad_down + grad.astype(jnp.float32))]
where the time goes in v1:
time: 160 us; the launch traced here: 159 us
  Pallas kernels  154 us (96%)
  local copies, waits for them, and re-layouts  4.97 us (3%)
    pallas_call x1, Pallas kernels, layer(): pl.pallas_call(functools.partial(layer_kernel, nz, tile), out_shape=(out,...  154 us
    unnamed x7, local copies, waits for them, and re-layouts  4.97 us

profile of v1, /device:TPU:0, one launch (start us, length us, event | category | flops | bytes accessed | tf_op | source)
XLA Modules:
  0.0 159.4 jit_solution(10792391473962414850)
XLA Ops:
  0.6 153.8 %layer_group.1 = (bf16[256,2048]{1,0:T(8,128)(2,1)}, bf16[256,2048]{1,0:T(8,128)(2,1)}, f32[2048,128]{1,0:T(8,128)}) custom-call(bf16[256,2048]{1,0:T(8,128)(2,1)} %x0.1, bf16[256,2048]{1,0:T(8,128)(2,1)} %x1.1, bf16[256,2048]{1,0:T(8,128)(2,1)} %x2.1, bf16[128,2048]{1,0:T(8,128)(2,1)} %wg.1, bf16[128,2048]{1,0:T(8,128)(2,1)} %wu.1, bf16[2048,128]{1,0:T(8,128)(2,1)} %wd.1, ...), custom_call_target="tpu_custom_call" | custom-call | tf_op jit(solution)/shard_map/layer_group/pallas_call | solution.py:497
  154.4 0.0 copy-start.1
  154.4 2.4 %copy.15 = bf16[256,2048]{1,0:T(8,128)(2,1)} copy(bf16[256,2048]{1,0:T(8,128)(2,1)} %get-tuple-element.6) | data formatting | bytes 2097152
  156.8 0.0 copy-done.1
  156.8 0.0 copy-start
  156.8 1.0 copy.16
  157.8 0.6 copy-done
  158.4 1.0 copy.17
Async XLA Ops:
  154.4 2.4 %copy-start.1 = (bf16[256,2048]{1,0:T(8,128)(2,1)S(1)}, bf16[256,2048]{1,0:T(8,128)(2,1)}, u32[]{:S(2)}) copy-start(bf16[256,2048]{1,0:T(8,128)(2,1)} %get-tuple-element.7) | copy-start | bytes 3145732
  156.8 1.6 %copy-start = (f32[2048,128]{1,0:T(8,128)S(1)}, f32[2048,128]{1,0:T(8,128)}, u32[]{:S(2)}) copy-start(f32[2048,128]{1,0:T(8,128)} %get-tuple-element.8) | copy-start | bytes 3145732

commit v2 on v1

--- a/solution.py
+++ b/solution.py
@@ -10,6 +10,7 @@
 GROUP = 4
 VMEM_BYTES = 63 * 1024 * 1024
 VMEM = pl.BlockSpec(memory_space=pltpu.VMEM)
+ANY = pl.BlockSpec(memory_space=pl.ANY)
 
 
 def place():
@@ -46,11 +47,11 @@
     return lax.dot_general(left, right, (dims, ((), ())), preferred_element_type=jnp.float32)
 
 
-def layer_kernel(nz, tile, x0, x1, x2, wg, wu, wd, taps, bias, gd, y, dx, g,
-                 t0, t1, t2, og, ou, od, hid, hid_t, conv_s, up_s, dup, dgate, yp, xp, gp,
-                 core, summed, got, gin_r, gin_l, gsum, hand,
+def layer_kernel(nz, tile, x0, x1, x2, wg, wu, wd, taps, bias, gd_in, y_out, dx_out, g_out,
+                 y, dx, g, gd, t0, t1, t2, og, ou, od, hid, hid_t, conv_s, up_s, dup, dgate, yp, xp, gp,
+                 core, summed, got, gin_r, gin_l, hand, passed_r, passed_l,
                  loc, w_s, w_r, n_s, n_r, p_s, p_r, r_s, r_r, l_s, l_r,
-                 c_s, c_r, a_s, a_r, zr_s, zr_r, zl_s, zl_r, g_s, g_r, e_s, e_r):
+                 c_s, c_r, a_s, a_r, zr_s, zr_r, zl_s, zl_r, g_s, g_r, pr_s, pr_r, pl_s, pl_r, fr_s, fr_r, fl_s, fl_r, e_s, e_r):
     f, c, q, z, qa, qb, qd = place()
     base = z * GROUP
     xs, ts, outs = (x0, x1, x2), (t0, t1, t2), (og, ou, od)
@@ -67,9 +68,10 @@
         pl.semaphore_signal(barrier, 1, device_id={"fs": base + peer}, device_id_type=pl.DeviceIdType.MESH)
     pl.semaphore_signal(barrier, 1, device_id={"tp": 1 - c}, device_id_type=pl.DeviceIdType.MESH)
     for s in range(1, nz):
-        pl.semaphore_signal(barrier, 1, device_id={"fs": lax.rem(z + s, nz) * GROUP + q},
-                            device_id_type=pl.DeviceIdType.MESH)
-    pl.semaphore_wait(barrier, 3 + nz)
+        for peer in range(GROUP):
+            pl.semaphore_signal(barrier, 1, device_id={"fs": lax.rem(z + s, nz) * GROUP + peer},
+                                device_id_type=pl.DeviceIdType.MESH)
+    pl.semaphore_wait(barrier, GROUP * nz)
 
     def piece(k, peer):
         if k == 2:
@@ -175,6 +177,9 @@
         copy = pltpu.make_async_copy(xs[i], ts[i].at[q], loc.at[3 + i])
         copy.start()
         local.append(copy)
+
+    old_grad = pltpu.make_async_copy(gd_in, gd, loc.at[6])
+    old_grad.start()
 
     row = lax.broadcasted_iota(jnp.int32, (rows, tile), 0)
 
@@ -205,6 +210,82 @@
 
     upper = lax.div(2 * z, nz)
 
+    def to_owners(o, into, send_sems, recv_sems, act):
+        for d, peer in enumerate((qa, qb, qd)):
+            src = gp.at[:, at(o * wide + peer * r, r)]
+            act(remote(src, into.at[at(q * u, u), :], send_sems.at[d], recv_sems.at[d], fs=base + peer))
+
+    def keep_own(o, into):
+        into[at(q * u, u), :] = gp[:, at(o * wide + q * r, r)]
+
+    def exchange(act):
+        to_owners(z, hand, g_s, g_r, act)
+
+    def passing_r(act):
+        to_owners(nz - 1, passed_r, pr_s, pr_r, act)
+
+    def passing_l(act):
+        to_owners(0, passed_l, pl_s, pl_r, act)
+
+    def passed_on_r():
+        return remote(passed_r, passed_r, fr_s.at[0], fr_r.at[0], fs=f + GROUP)
+
+    def passed_on_l():
+        return remote(passed_l, passed_l, fl_s.at[0], fl_r.at[0], fs=f - GROUP)
+
+    arrival = lambda copy: copy.wait_recv()
+
+    def hand_on():
+        @pl.when(z == nz - 2)
+        def _():
+            passing_r(arrival)
+            passed_on_r().start()
+
+        @pl.when(z == 1)
+        def _():
+            passing_l(arrival)
+            passed_on_l().start()
+
+    def slot_r(o, m):
+        return remote(gp.at[:, at(o * wide, wide)], gin_r.at[m], zr_s.at[m], zr_r.at[m], fs=f + GROUP)
+
+    def slot_l(o, m):
+        return remote(gp.at[:, at(o * wide, wide)], gin_l.at[m], zl_s.at[m], zl_r.at[m], fs=f - GROUP)
+
+    def rightward(o, m, act=begin):
+        if m < nz - 2:
+            act(slot_r(o, m))
+            return
+
+        @pl.when(z == nz - 2)
+        def _():
+            passing_r(act)
+            if act is begin:
+                keep_own(nz - 1, passed_r)
+            else:
+                act(passed_on_r())
+
+        @pl.when(z < nz - 2)
+        def _():
+            act(slot_r(o, m))
+
+    def leftward(o, m, act=begin):
+        if m < nz - 2:
+            act(slot_l(o, m))
+            return
+
+        @pl.when(z == 1)
+        def _():
+            passing_l(act)
+            if act is begin:
+                keep_own(0, passed_l)
+            else:
+                act(passed_on_l())
+
+        @pl.when(z > 1)
+        def _():
+            act(slot_l(o, m))
+
     def down_grad():
         for i in range(nz):
             o = nz - 1 - i + upper * (2 * i - (nz - 1))
@@ -214,59 +295,57 @@
             if i < nz - 1:
                 @pl.when(low)
                 def _():
-                    remote(gp.at[:, cols], gin_r.at[i], zr_s.at[i], zr_r.at[i], fs=f + GROUP).start()
+                    rightward(o, i)
 
                 @pl.when(high)
                 def _():
-                    remote(gp.at[:, cols], gin_l.at[i], zl_s.at[i], zl_r.at[i], fs=f - GROUP).start()
-
-    def gone(i):
-        cols = at((nz - 1 - i) * wide, wide)
-        return remote(gp.at[:, cols], gin_r.at[i], zr_s.at[i], zr_r.at[i], fs=f + GROUP)
+                    leftward(o, i)
+
+        @pl.when(jnp.logical_or(low, high))
+        def _():
+            exchange(begin)
+
+    def settle():
+        @pl.when(jnp.logical_and(first, last))
+        def _():
+            m = nz - 2
+            slot_r(z, m).wait_recv()
+            slot_l(z, m).wait_recv()
+            home = gp.at[:, at(z * wide, wide)]
+            total(home, [home, gin_r.at[m], gin_l.at[m]], u)
+            exchange(begin)
 
     def chain(j):
         o = nz - 2 + z - j
-        got_r = remote(gin_r.at[j], gin_r.at[j], zr_s.at[j], zr_r.at[j], fs=f - GROUP)
-        got_l = remote(gin_l.at[j], gin_l.at[j], zl_s.at[j], zl_r.at[j], fs=f + GROUP)
 
         @pl.when(jnp.logical_and(first, o <= nz - 1))
         def _():
-            got_r.wait_recv()
-
-        if j < nz - 2:
-            @pl.when(jnp.logical_and(first, o <= nz - 1))
-            def _():
-                cols = at(o * wide, wide)
-                total(gp.at[:, cols], [gp.at[:, cols], gin_r.at[j]], u)
-                remote(gp.at[:, cols], gin_r.at[j + 1], zr_s.at[j + 1], zr_r.at[j + 1], fs=f + GROUP).start()
-
-        p = z + 1 - nz + 1 + j
+            slot_r(o, j).wait_recv()
+            cols = at(o * wide, wide)
+            total(gp.at[:, cols], [gp.at[:, cols], gin_r.at[j]], u)
+            rightward(o, j + 1)
+
+        p = z + 2 - nz + j
 
         @pl.when(jnp.logical_and(last, p >= 0))
         def _():
-            got_l.wait_recv()
-
-        if j < nz - 2:
-            @pl.when(jnp.logical_and(last, p >= 0))
-            def _():
-                cols = at(p * wide, wide)
-                total(gp.at[:, cols], [gp.at[:, cols], gin_l.at[j]], u)
-                remote(gp.at[:, cols], gin_l.at[j + 1], zl_s.at[j + 1], zl_r.at[j + 1], fs=f - GROUP).start()
-
-    def backward():
-        @pl.loop(0, GROUP)
-        def _(b):
-            @pl.loop(0, u // tile)
-            def _(j):
-                cols, seq, par = at(j * tile, tile), at(b * rows, rows), at(units + j * tile, tile)
-                dh = mm(t2[b], od[at(j * tile, tile), :], ((1,), (1,)))
-                conv = conv_s[seq, cols]
-                sig = 1.0 / (1.0 + jnp.exp(-conv))
-                dup[seq, cols] = (dh * (conv * sig)).astype(jnp.bfloat16)
-                dc = dh * up_s[seq, cols] * sig * (1.0 + conv * (1.0 - sig))
-                dg = (taps[2:3, par] * dc + taps[1:2, par] * earlier(dc, 1)
-                      + taps[0:1, par] * earlier(dc, 2))
-                dgate[seq, cols] = dg.astype(jnp.bfloat16)
+            slot_l(p, j).wait_recv()
+            cols = at(p * wide, wide)
+            total(gp.at[:, cols], [gp.at[:, cols], gin_l.at[j]], u)
+            leftward(p, j + 1)
+
+    def backward(b):
+        @pl.loop(0, u // tile)
+        def _(j):
+            cols, seq, par = at(j * tile, tile), at(b * rows, rows), at(units + j * tile, tile)
+            dh = mm(t2[b], od[at(j * tile, tile), :], ((1,), (1,)))
+            conv = conv_s[seq, cols]
+            sig = 1.0 / (1.0 + jnp.exp(-conv))
+            dup[seq, cols] = (dh * (conv * sig)).astype(jnp.bfloat16)
+            dc = dh * up_s[seq, cols] * sig * (1.0 + conv * (1.0 - sig))
+            dg = (taps[2:3, par] * dc + taps[1:2, par] * earlier(dc, 1)
+                  + taps[0:1, par] * earlier(dc, 2))
+            dgate[seq, cols] = dg.astype(jnp.bfloat16)
 
     mirrored = z + upper * (nz - 1 - 2 * z)
 
@@ -285,66 +364,90 @@
             cols = at(start + j * sub, sub)
             yp[:, cols] = mm(hid[...], od[:, cols]).astype(jnp.bfloat16)
 
-    def early_block(i):
-        @pl.loop(0, wide // sub)
-        def _(j):
-            cols = at(i * wide + j * sub, sub)
-            part = mm(dup[...], ou[cols, :], ((1,), (1,))) + mm(dgate[...], og[cols, :], ((1,), (1,)))
-            xp[:, cols] = part.astype(jnp.bfloat16)
-
     parts, finals = (yp, xp), (y, dx)
     order = (qd, qa, qb, q)
     theirs = (qd, qb, qa, q)
-    cores, sends, ends = {}, {}, []
 
     def span(t, i):
         return at(turn(i) * wide, wide) if t == 0 else at(i * wide, wide)
 
+    def core_copy(t, i, n):
+        cols = span(t, i)
+        src = parts[t].at[at(theirs[n] * rows + (1 - c) * half, half), cols]
+        return remote(src, core.at[t, n, :, cols], c_s.at[t, i, n], c_r.at[t, i, n], tp=1 - c)
+
     def to_core(t, i):
+        for n in range(4):
+            core_copy(t, i, n).start()
+
+    def plane_copy(t, i, slot):
         cols = span(t, i)
+        src = core.at[t, 0, :, cols] if slot == 2 else summed.at[t, slot, :, cols]
+        return remote(src, got.at[t, slot, :, cols], a_s.at[t, i, slot], a_r.at[t, i, slot],
+                      fs=base + (qb if slot == 2 else qa))
+
+    def join_one(t, i, n):
+        cols = span(t, i)
+        core_copy(t, i, n).wait_recv()
+        own = parts[t].at[at(order[n] * rows + c * half, half), cols]
+        total(summed.at[t, n, :, cols], [own, core.at[t, n, :, cols]], half)
+        if n < 2:
+            plane_copy(t, i, n).start()
+
+    def join(t, i):
         for n in range(4):
-            src = parts[t].at[at(theirs[n] * rows + (1 - c) * half, half), cols]
-            copy = remote(src, core.at[t, n, :, cols], c_s.at[t, i, n], c_r.at[t, i, n], tp=1 - c)
-            copy.start()
-            cores[t, i, n] = copy
-
-    def send(t, i, src, slot, peer):
-        cols = span(t, i)
-        copy = remote(src, got.at[t, slot, :, cols], a_s.at[t, i, slot], a_r.at[t, i, slot], fs=base + peer)
-        copy.start()
-        sends[t, i, slot] = copy
-
-    def join(t, i):
-        cols = span(t, i)
-        for n in range(4):
-            cores[t, i, n].wait_recv()
-            own = parts[t].at[at(order[n] * rows + c * half, half), cols]
-            total(summed.at[t, n, :, cols], [own, core.at[t, n, :, cols]], half)
-            if n < 2:
-                send(t, i, summed.at[t, n, :, cols], n, qa)
+            join_one(t, i, n)
 
     def second(t, i):
         cols = span(t, i)
-        sends[t, i, 0].wait_recv()
+        plane_copy(t, i, 0).wait_recv()
         total(core.at[t, 0, :, cols], [summed.at[t, 2, :, cols], got.at[t, 0, :, cols]], half)
-        send(t, i, core.at[t, 0, :, cols], 2, qb)
+        plane_copy(t, i, 2).start()
+
+    def end_copy(t, i):
+        there = finals[t].at[mine, span(t, i)]
+        return remote(there, there, e_s.at[t, i], e_r.at[t, i], tp=1 - c)
 
     def finish(t, i):
         cols = span(t, i)
-        sends[t, i, 1].wait_recv()
-        sends[t, i, 2].wait_recv()
-        there = finals[t].at[mine, cols]
-        total(there, [summed.at[t, 3, :, cols], got.at[t, 1, :, cols], got.at[t, 2, :, cols]], half)
-        copy = remote(there, there, e_s.at[t, i], e_r.at[t, i], tp=1 - c)
-        copy.start()
-        ends.append(copy)
-
-    stages = (to_core, join, second, finish)
-
-    def step(t, i, *which):
+        plane_copy(t, i, 1).wait_recv()
+        plane_copy(t, i, 2).wait_recv()
+        total(finals[t].at[mine, cols], [summed.at[t, 3, :, cols], got.at[t, 1, :, cols], got.at[t, 2, :, cols]], half)
+        end_copy(t, i).start()
+
+    def each(fn):
+        @pl.loop(0, nz)
+        def _(i):
+            fn(i)
+
+    def early_out(owner, n):
+        seq = at(owner * rows, rows)
+
+        @pl.loop(0, nz)
+        def _(i):
+            cols = at(i * wide, wide)
+            part = mm(dup[seq, :], ou[cols, :], ((1,), (1,))) + mm(dgate[seq, :], og[cols, :], ((1,), (1,)))
+            xp[seq, cols] = part.astype(jnp.bfloat16)
+            core_copy(1, i, n).start()
+
+    def joins(n):
+        each(lambda i: join_one(1, i, n))
+
+    def seconds():
+        each(lambda i: second(1, i))
+
+    def finishes(t):
+        each(lambda i: finish(t, i))
+
+    def ended_out(t):
+        each(lambda i: end_copy(t, i).wait_recv())
+
+    stages = (to_core, join, second)
+
+    def step(i, *which):
         for s in which:
             if 0 <= i - s < nz:
-                stages[s](t, i - s)
+                stages[s](0, i - s)
 
     partner, far = [], {}
 
@@ -409,79 +512,124 @@
     for s in range(1, nz - 2):
         relay(2, s)
 
-    for i in range(nz):
-        if i == nz - 1 and nz > 2:
-            chain(0)
+    for i in range(nz - 1):
         if i > 0:
             ended(2, i - 1)
         late_block(i)
-        step(0, i, 0, 1, 2)
-    backward()
-    step(0, nz, 1, 2)
-    early_block(0)
-    step(1, 0, 0)
-    step(0, nz + 1, 2)
-    for i in range(1, nz):
-        early_block(i)
-        step(1, i, 0, 1)
+        step(i, 0, 1, 2)
+    step(nz - 1, 1)
+    if nz > 2:
+        chain(0)
+    step(nz - 1, 2)
+    if nz > 1:
+        ended(2, nz - 2)
+    late_block(nz - 1)
+    to_core(0, nz - 1)
+    backward(qd)
+    step(nz, 1)
+    early_out(qd, 0)
+    step(nz, 2)
+    backward(qa)
+    joins(0)
+    early_out(qa, 2)
+    backward(qb)
+    early_out(qb, 1)
+    step(nz + 1, 2)
+    joins(2)
     for j in range(1, nz - 2):
         chain(j)
-    for i in range(nz):
-        finish(0, i)
-    step(1, nz, 1)
-    for i in range(nz):
-        second(1, i)
-        if i == min(1, nz - 1):
-            if nz > 1:
-                chain(nz - 2)
-            home = gp.at[:, at(z * wide, wide)]
-            if nz == 1:
-                total(gsum, [home], u)
-            else:
-                lo_in, hi_in = gin_r.at[nz - 2], gin_l.at[nz - 2]
-                for cond, srcs in ((low, [home, hi_in]), (high, [home, lo_in]),
-                                   (jnp.logical_and(first, last), [home, lo_in, hi_in])):
-                    @pl.when(cond)
-                    def _(srcs=srcs):
-                        total(gsum, srcs, u)
-            handed = []
-            for d, peer in enumerate((qa, qb, qd)):
-                copy = remote(gsum.at[:, at(peer * r, r)], hand.at[at(q * u, u), :], g_s.at[d], g_r.at[d],
-                              fs=base + peer)
-                copy.start()
-                handed.append(copy)
-            hand[at(q * u, u), :] = gsum[:, at(q * r, r)]
-        if i > 0:
-            finish(1, i - 1)
-    finish(1, nz - 1)
-    for copy in handed:
-        copy.wait_recv()
-
-    @pl.loop(0, GROUP * u, step=128)
-    def _(i):
-        sl = at(i, 128)
-        g[sl, :] = gd[sl, :] + hand[sl, :].astype(jnp.float32)
-
-    for copy in ends:
-        copy.wait_recv()
-    for copies in (weights, near, far, cores, sends):
+    backward(q)
+    joins(1)
+    early_out(q, 3)
+    seconds()
+    if nz > 1:
+        hand_on()
+        settle()
+    joins(3)
+    finishes(0)
+    ended_out(0)
+    y_copy = pltpu.make_async_copy(y, y_out, loc.at[7])
+    y_copy.start()
+    finishes(1)
+    exchange(arrival)
+    keep_own(z, hand)
+    if nz > 1:
+        @pl.when(high)
+        def _():
+            passed_on_r().wait_recv()
+
+        @pl.when(low)
+        def _():
+            passed_on_l().wait_recv()
+
+    old_grad.wait()
+
+    def grad_sum(*extra):
+        @pl.loop(0, GROUP * u, step=128)
+        def _(i):
+            sl = at(i, 128)
+            out = hand[sl, :].astype(jnp.float32)
+            for e in extra:
+                out = out + e[sl, :].astype(jnp.float32)
+            g[sl, :] = gd[sl, :] + out
+
+    inner = jnp.logical_and(first, last) if nz > 1 else low
+
+    @pl.when(inner)
+    def _():
+        grad_sum()
+
+    if nz > 1:
+        @pl.when(high)
+        def _():
+            grad_sum(passed_r)
+
+        @pl.when(low)
+        def _():
+            grad_sum(passed_l)
+
+    g_copy = pltpu.make_async_copy(g, g_out, loc.at[8])
+    g_copy.start()
+    ended_out(1)
+    dx_copy = pltpu.make_async_copy(dx, dx_out, loc.at[9])
+    dx_copy.start()
+    for copies in (weights, near, far):
         for copy in copies.values():
             copy.wait_send()
-    for copy in partner + handed + ends:
+    for copy in partner:
         copy.wait_send()
+    exchange(sent)
+    for t in range(2):
+        @pl.loop(0, nz)
+        def _(i, t=t):
+            for n in range(4):
+                core_copy(t, i, n).wait_send()
+            for slot in range(3):
+                plane_copy(t, i, slot).wait_send()
+            end_copy(t, i).wait_send()
     for s in range(nz - 1):
         for k in range(3):
             onward(k, s, sent)
-    for m in range(nz - 1):
-        chunk = gp.at[:, at(0, wide)]
-
+    for m in range(nz - 2):
         @pl.when(jnp.logical_and(last, z <= m))
-        def _():
-            remote(chunk, gin_r.at[m], zr_s.at[m], zr_r.at[m], fs=f + GROUP).wait_send()
+        def _(m=m):
+            rightward(0, m, sent)
 
         @pl.when(jnp.logical_and(first, nz - 1 - z <= m))
-        def _():
-            remote(chunk, gin_l.at[m], zl_s.at[m], zl_r.at[m], fs=f - GROUP).wait_send()
+        def _(m=m):
+            leftward(0, m, sent)
+
+    if nz > 1:
+        @pl.when(last)
+        def _():
+            rightward(0, nz - 2, sent)
+
+        @pl.when(first)
+        def _():
+            leftward(0, nz - 2, sent)
+
+    for copy in (y_copy, g_copy, dx_copy):
+        copy.wait()
 
 
 def layer(nz, xs, w_gate, w_up, w_down, taps, bias, grad_down):
@@ -497,20 +645,23 @@
     return pl.pallas_call(
         functools.partial(layer_kernel, nz, tile),
         out_shape=(out, out, jax.ShapeDtypeStruct((u * GROUP, r), f32)),
-        in_specs=[VMEM] * 9,
-        out_specs=(VMEM,) * 3,
-        scratch_shapes=[pltpu.VMEM((GROUP, rows, d), b16)] * 3
+        in_specs=[ANY] * 6 + [VMEM] * 2 + [ANY],
+        out_specs=(ANY,) * 3,
+        scratch_shapes=[pltpu.VMEM((rows, d), b16)] * 2
+        + [pltpu.VMEM((u * GROUP, r), f32)] * 2
+        + [pltpu.VMEM((GROUP, rows, d), b16)] * 3
         + [pltpu.VMEM((d, u), b16)] * 2
         + [pltpu.VMEM((u, d), b16), pltpu.VMEM((toks, u), b16), pltpu.VMEM((u, toks), b16),
            pltpu.VMEM((toks, u), f32), pltpu.VMEM((toks, u), f32),
            pltpu.VMEM((toks, u), b16), pltpu.VMEM((toks, u), b16),
            pltpu.VMEM((toks, d), b16), pltpu.VMEM((toks, d), b16), pltpu.VMEM((u, d), b16),
            pltpu.VMEM((2, 4, half, d), b16), pltpu.VMEM((2, 4, half, d), b16), pltpu.VMEM((2, 3, half, d), b16),
-           pltpu.VMEM((hops, u, wide), b16), pltpu.VMEM((hops, u, wide), b16),
-           pltpu.VMEM((u, wide), b16), pltpu.VMEM((u * GROUP, r), b16),
-           pltpu.SemaphoreType.DMA((6,))]
+           pltpu.VMEM((hops, u, wide), b16), pltpu.VMEM((hops, u, wide), b16)]
+        + [pltpu.VMEM((u * GROUP, r), b16)] * 3
+        + [pltpu.SemaphoreType.DMA((10,))]
         + sems(3, 3) + sems(3, 3) + sems(3, 3) + sems(hops, 3) + sems(hops, 3)
-        + sems(2, nz, 4) + sems(2, nz, 3) + sems(hops) + sems(hops) + sems(3) + sems(2, nz),
+        + sems(2, nz, 4) + sems(2, nz, 3) + sems(hops) + sems(hops) + sems(3)
+        + sems(3) + sems(3) + sems(1) + sems(1) + sems(2, nz),
         compiler_params=pltpu.CompilerParams(collective_id=0, has_side_effects=True, vmem_limit_bytes=VMEM_BYTES),
         name="layer_group",
     )(*xs, w_gate, w_up, w_down, taps, bias, grad_down)

time: 160 us -> 149 us (0.931)
  Pallas kernels: 154 us -> 142 us
    pallas_call x1, Pallas kernels: 154 us -> 142 us  [layer(): pl.pallas_call(functools.partial(layer_kernel, nz, tile), out_shape=(out,...]
where the time goes in v2:
time: 149 us; the launch traced here: 148 us
  Pallas kernels  142 us (95%)
  local copies, waits for them, and re-layouts  4.97 us (3%)
    pallas_call x1, Pallas kernels, layer(): pl.pallas_call(functools.partial(layer_kernel, nz, tile), out_shape=(out,...  142 us
    unnamed x7, local copies, waits for them, and re-layouts  4.97 us

profile of v2, /device:TPU:0, one launch (start us, length us, event | category | flops | bytes accessed | tf_op | source)
XLA Modules:
  0.0 147.8 jit_solution(536595827620853738)
XLA Ops:
  0.6 142.2 %layer_group.1 = (bf16[256,2048]{1,0:T(8,128)(2,1)}, bf16[256,2048]{1,0:T(8,128)(2,1)}, f32[2048,128]{1,0:T(8,128)}) custom-call(bf16[256,2048]{1,0:T(8,128)(2,1)} %x0.1, bf16[256,2048]{1,0:T(8,128)(2,1)} %x1.1, bf16[256,2048]{1,0:T(8,128)(2,1)} %x2.1, bf16[128,2048]{1,0:T(8,128)(2,1)} %wg.1, bf16[128,2048]{1,0:T(8,128)(2,1)} %wu.1, bf16[2048,128]{1,0:T(8,128)(2,1)} %wd.1, ...), custom_call_target="tpu_custom_call" | custom-call | tf_op jit(solution)/shard_map/layer_group/pallas_call | solution.py:645
  142.8 0.0 copy-start.1
  142.8 2.4 %copy.15 = bf16[256,2048]{1,0:T(8,128)(2,1)} copy(bf16[256,2048]{1,0:T(8,128)(2,1)} %get-tuple-element.6) | data formatting | bytes 2097152
  145.2 0.0 copy-done.1
  145.2 0.0 copy-start
  145.2 1.0 copy.16
  146.2 0.6 copy-done
  146.8 1.0 copy.17
Async XLA Ops:
  142.8 2.4 %copy-start.1 = (bf16[256,2048]{1,0:T(8,128)(2,1)S(1)}, bf16[256,2048]{1,0:T(8,128)(2,1)}, u32[]{:S(2)}) copy-start(bf16[256,2048]{1,0:T(8,128)(2,1)} %get-tuple-element.7) | copy-start | bytes 3145732
  145.2 1.6 %copy-start = (f32[2048,128]{1,0:T(8,128)S(1)}, f32[2048,128]{1,0:T(8,128)}, u32[]{:S(2)}) copy-start(f32[2048,128]{1,0:T(8,128)} %get-tuple-element.8) | copy-start | bytes 3145732

commit v3 on v2

--- a/solution.py
+++ b/solution.py
@@ -48,10 +48,10 @@
 
 
 def layer_kernel(nz, tile, x0, x1, x2, wg, wu, wd, taps, bias, gd_in, y_out, dx_out, g_out,
-                 y, dx, g, gd, t0, t1, t2, og, ou, od, hid, hid_t, conv_s, up_s, dup, dgate, yp, xp, gp,
+                 y, dx, g, gd, t0, t1, t2, og, ou, od, hid, hid_t, conv_s, up_s, gate_l, up_l, dup, dgate, yp, xp, gp,
                  core, summed, got, gin_r, gin_l, hand, passed_r, passed_l,
                  loc, w_s, w_r, n_s, n_r, p_s, p_r, r_s, r_r, l_s, l_r,
-                 c_s, c_r, a_s, a_r, zr_s, zr_r, zl_s, zl_r, g_s, g_r, pr_s, pr_r, pl_s, pl_r, fr_s, fr_r, fl_s, fl_r, e_s, e_r):
+                 c_s, c_r, a_s, a_r, zr_s, zr_r, zl_s, zl_r, g_s, g_r, pr_s, pr_r, pl_s, pl_r, fr_s, fr_r, fl_s, fl_r, e_s, e_r, o_s):
     f, c, q, z, qa, qb, qd = place()
     base = z * GROUP
     xs, ts, outs = (x0, x1, x2), (t0, t1, t2), (og, ou, od)
@@ -59,6 +59,8 @@
     half = rows // 2
     r, u = wg.shape[0], og.shape[1]
     wide = GROUP * r
+    parts_d = wide // 256 if wide % 256 == 0 else 1
+    part, downs = wide // parts_d, range(2, 2 + parts_d)
     first, last = z > 0, z < nz - 1
     low, high = z == 0, z == nz - 1
     units = (c * GROUP + q) * u
@@ -67,11 +69,16 @@
     for peer in (qa, qb, qd):
         pl.semaphore_signal(barrier, 1, device_id={"fs": base + peer}, device_id_type=pl.DeviceIdType.MESH)
     pl.semaphore_signal(barrier, 1, device_id={"tp": 1 - c}, device_id_type=pl.DeviceIdType.MESH)
-    for s in range(1, nz):
-        for peer in range(GROUP):
-            pl.semaphore_signal(barrier, 1, device_id={"fs": lax.rem(z + s, nz) * GROUP + peer},
-                                device_id_type=pl.DeviceIdType.MESH)
-    pl.semaphore_wait(barrier, GROUP * nz)
+    @pl.when(last)
+    def _():
+        pl.semaphore_signal(barrier, 1, device_id={"fs": f + GROUP}, device_id_type=pl.DeviceIdType.MESH)
+
+    @pl.when(first)
+    def _():
+        pl.semaphore_signal(barrier, 1, device_id={"fs": f - GROUP}, device_id_type=pl.DeviceIdType.MESH)
+
+    beside = lax.div(z + nz - 1, nz) + lax.div(2 * nz - 2 - z, nz)
+    pl.semaphore_wait(barrier, GROUP + beside)
 
     def piece(k, peer):
         if k == 2:
@@ -84,8 +91,8 @@
         return outs[k].at[at(owner * r, r), :]
 
     def block(k, b):
-        if k == 2:
-            return od.at[:, at(b * wide, wide)]
+        if k >= 2:
+            return od.at[:, at(b * wide + (k - 2) * part, part)]
         return outs[k].at[at(b * wide, wide), :]
 
     def right(k, s):
@@ -189,15 +196,39 @@
     def earlier(v, steps):
         return jnp.where(row < rows - steps, pltpu.roll(v, rows - steps, 0), 0.0)
 
-    def forward(t, keep):
+    upper = lax.div(2 * z, nz)
+    head_k = pl.ds(pl.multiple_of(upper * wide, wide), max(nz - 1, 1) * wide)
+    tail_k = at((1 - upper) * (nz - 1) * wide, wide)
+
+    def begun(i):
+        t, kept_gate, kept_up = ((t0, gate_l, up_l), (t1, conv_s, up_s))[i]
+
+        @pl.loop(0, GROUP)
+        def _(b):
+            @pl.loop(0, u // tile)
+            def _(j):
+                cols, seq = at(j * tile, tile), at(b * rows, rows)
+                x = t[b, :, head_k]
+                kept_gate[seq, cols] = mm(x, og[head_k, cols])
+                kept_up[seq, cols] = mm(x, ou[head_k, cols])
+
+    def forward(i, split):
+        t, kept_gate, kept_up = ((t0, gate_l, up_l), (t1, conv_s, up_s))[i]
+        keep = i == 1
+
         @pl.loop(0, GROUP)
         def _(b):
             @pl.loop(0, u // tile)
             def _(j):
                 cols, seq, par = at(j * tile, tile), at(b * rows, rows), at(units + j * tile, tile)
-                x = t[b]
-                gate = mm(x, og[:, cols]).astype(jnp.bfloat16).astype(jnp.float32)
-                up = mm(x, ou[:, cols])
+                if split:
+                    x = t[b, :, tail_k]
+                    gate = kept_gate[seq, cols] + mm(x, og[tail_k, cols])
+                    up = kept_up[seq, cols] + mm(x, ou[tail_k, cols])
+                else:
+                    x = t[b]
+                    gate, up = mm(x, og[:, cols]), mm(x, ou[:, cols])
+                gate = gate.astype(jnp.bfloat16).astype(jnp.float32)
                 conv = (bias[:, par] + taps[2:3, par] * gate + taps[1:2, par] * later(gate, 1)
                         + taps[0:1, par] * later(gate, 2))
                 out = conv / (1.0 + jnp.exp(-conv)) * up
@@ -207,8 +238,6 @@
                     hid_t[at(j * tile, tile), seq] = out.T.astype(jnp.bfloat16)
                 else:
                     hid[seq, cols] = out.astype(jnp.bfloat16)
-
-    upper = lax.div(2 * z, nz)
 
     def to_owners(o, into, send_sems, recv_sems, act):
         for d, peer in enumerate((qa, qb, qd)):
@@ -334,18 +363,20 @@
             total(gp.at[:, cols], [gp.at[:, cols], gin_l.at[j]], u)
             leftward(p, j + 1)
 
-    def backward(b):
+    def backward(n):
+        b, out = order[n], pl.ds(n * rows, rows)
+
         @pl.loop(0, u // tile)
         def _(j):
             cols, seq, par = at(j * tile, tile), at(b * rows, rows), at(units + j * tile, tile)
             dh = mm(t2[b], od[at(j * tile, tile), :], ((1,), (1,)))
             conv = conv_s[seq, cols]
             sig = 1.0 / (1.0 + jnp.exp(-conv))
-            dup[seq, cols] = (dh * (conv * sig)).astype(jnp.bfloat16)
+            dup[out, cols] = (dh * (conv * sig)).astype(jnp.bfloat16)
             dc = dh * up_s[seq, cols] * sig * (1.0 + conv * (1.0 - sig))
             dg = (taps[2:3, par] * dc + taps[1:2, par] * earlier(dc, 1)
                   + taps[0:1, par] * earlier(dc, 2))
-            dgate[seq, cols] = dg.astype(jnp.bfloat16)
+            dgate[out, cols] = dg.astype(jnp.bfloat16)
 
     mirrored = z + upper * (nz - 1 - 2 * z)
 
@@ -354,26 +385,26 @@
         v = i + near_side * (mirrored - 2 * i)
         return v + upper * (nz - 1 - 2 * v)
 
-    sub = 256 if wide % 256 == 0 else 128
-
-    def late_block(i):
-        start = turn(i) * wide
-
-        @pl.loop(0, wide // sub)
-        def _(j):
-            cols = at(start + j * sub, sub)
-            yp[:, cols] = mm(hid[...], od[:, cols]).astype(jnp.bfloat16)
-
-    parts, finals = (yp, xp), (y, dx)
+
+    def late_start(h):
+        return turn(h // parts_d) * wide + h % parts_d * part if isinstance(h, int) else (
+            turn(lax.div(h, parts_d)) * wide + lax.rem(h, parts_d) * part)
+
+    def late_block(h):
+        cols = at(late_start(h), part)
+        yp[:, cols] = mm(hid[...], od[:, cols]).astype(jnp.bfloat16)
+
+    parts, finals, results = (yp, xp), (y, dx), (y_out, dx_out)
     order = (qd, qa, qb, q)
     theirs = (qd, qb, qa, q)
+    places = ((order, theirs), ((0, 1, 2, 3), (0, 2, 1, 3)))
 
     def span(t, i):
-        return at(turn(i) * wide, wide) if t == 0 else at(i * wide, wide)
+        return at(late_start(i), part) if t == 0 else at(i * wide, wide)
 
     def core_copy(t, i, n):
         cols = span(t, i)
-        src = parts[t].at[at(theirs[n] * rows + (1 - c) * half, half), cols]
+        src = parts[t].at[at(places[t][1][n] * rows + (1 - c) * half, half), cols]
         return remote(src, core.at[t, n, :, cols], c_s.at[t, i, n], c_r.at[t, i, n], tp=1 - c)
 
     def to_core(t, i):
@@ -389,7 +420,7 @@
     def join_one(t, i, n):
         cols = span(t, i)
         core_copy(t, i, n).wait_recv()
-        own = parts[t].at[at(order[n] * rows + c * half, half), cols]
+        own = parts[t].at[at(places[t][0][n] * rows + c * half, half), cols]
         total(summed.at[t, n, :, cols], [own, core.at[t, n, :, cols]], half)
         if n < 2:
             plane_copy(t, i, n).start()
@@ -405,49 +436,63 @@
         plane_copy(t, i, 2).start()
 
     def end_copy(t, i):
-        there = finals[t].at[mine, span(t, i)]
-        return remote(there, there, e_s.at[t, i], e_r.at[t, i], tp=1 - c)
+        cols = span(t, i)
+        return remote(finals[t].at[:, cols], results[t].at[mine, cols], e_s.at[t, i], e_r.at[t, i], tp=1 - c)
+
+    def own_copy(t, i):
+        cols = span(t, i)
+        return pltpu.make_async_copy(finals[t].at[:, cols], results[t].at[mine, cols], o_s.at[t, i])
 
     def finish(t, i):
         cols = span(t, i)
         plane_copy(t, i, 1).wait_recv()
         plane_copy(t, i, 2).wait_recv()
-        total(finals[t].at[mine, cols], [summed.at[t, 3, :, cols], got.at[t, 1, :, cols], got.at[t, 2, :, cols]], half)
+        total(finals[t].at[:, cols], [summed.at[t, 3, :, cols], got.at[t, 1, :, cols], got.at[t, 2, :, cols]], half)
         end_copy(t, i).start()
-
-    def each(fn):
-        @pl.loop(0, nz)
+        own_copy(t, i).start()
+
+    blocks = (nz * parts_d, nz)
+
+    def each(fn, t=1):
+        @pl.loop(0, blocks[t])
         def _(i):
             fn(i)
 
-    def early_out(owner, n):
-        seq = at(owner * rows, rows)
-
-        @pl.loop(0, nz)
-        def _(i):
-            cols = at(i * wide, wide)
-            part = mm(dup[seq, :], ou[cols, :], ((1,), (1,))) + mm(dgate[seq, :], og[cols, :], ((1,), (1,)))
-            xp[seq, cols] = part.astype(jnp.bfloat16)
-            core_copy(1, i, n).start()
+    def early_piece(n, m, i):
+        seq, cols = pl.ds(n * rows, m * rows), at(i * wide, wide)
+        out = mm(dup[seq, :], ou[cols, :], ((1,), (1,))) + mm(dgate[seq, :], og[cols, :], ((1,), (1,)))
+        xp[seq, cols] = out.astype(jnp.bfloat16)
+        for k in range(n, n + m):
+            core_copy(1, i, (0, 2, 1, 3)[k]).start()
+
+    def first_out():
+        for i in range(nz + 2):
+            if i < nz:
+                early_piece(0, 1, i)
+            if i > 1:
+                join_one(1, i - 2, 0)
+
+    def pair_out():
+        for i in range(nz + 1):
+            if i < nz:
+                early_piece(1, 2, i)
+            if i > 0:
+                join_one(1, i - 1, 2)
+                join_one(1, i - 1, 1)
+            if 1 < i < nz:
+                second(1, i - 2)
+
+    def last_out():
+        each(lambda i: early_piece(3, 1, i))
 
     def joins(n):
         each(lambda i: join_one(1, i, n))
 
-    def seconds():
-        each(lambda i: second(1, i))
-
     def finishes(t):
-        each(lambda i: finish(t, i))
+        each(lambda i: finish(t, i), t)
 
     def ended_out(t):
-        each(lambda i: end_copy(t, i).wait_recv())
-
-    stages = (to_core, join, second)
-
-    def step(i, *which):
-        for s in which:
-            if 0 <= i - s < nz:
-                stages[s](0, i - s)
+        each(lambda i: end_copy(t, i).wait_recv(), t)
 
     partner, far = [], {}
 
@@ -493,63 +538,124 @@
     for s in range(1, nz - 2):
         relay(0, s)
         relay(1, s)
-    onward(2, 0, begin)
+    for k in downs:
+        onward(k, 0, begin)
     adjacent(2)
+    at_end = jnp.logical_or(low, high) if nz > 1 else z < 0
+    inside = jnp.logical_and(first, last) if nz > 1 else z >= 0
+
+    def forward_head(i):
+        @pl.when(at_end)
+        def _():
+            begun(i)
+
+        @pl.when(inside)
+        def _():
+            forward(i, False)
+
+    def forward_tail(i):
+        @pl.when(at_end)
+        def _():
+            forward(i, True)
+
     opposite(1)
-    opposite(0)
     complete(1)
-    for s in range(nz - 1):
+    for s in range(nz - 2):
         ended(0, s)
         ended(1, s)
-    forward(t1, True)
     if nz > 2:
-        relay(2, 0)
+        for k in downs:
+            relay(k, 0)
+    forward_head(1)
+    opposite(0)
+    complete(0)
+    forward_head(0)
+    for s in range(1, nz - 2):
+        for k in downs:
+            relay(k, s)
+    if nz > 1:
+        ended(0, nz - 2)
+        ended(1, nz - 2)
+    forward_tail(1)
     opposite(2)
     complete(2)
     down_grad()
-    complete(0)
-    forward(t0, False)
-    for s in range(1, nz - 2):
-        relay(2, s)
-
-    for i in range(nz - 1):
-        if i > 0:
-            ended(2, i - 1)
-        late_block(i)
-        step(i, 0, 1, 2)
-    step(nz - 1, 1)
+    forward_tail(0)
+
+    count = blocks[0]
+
+    @pl.when(at_end)
+    def _():
+        progress = [0, 0]
+
+        def catch_up(stage, upto):
+            while progress[stage] <= upto:
+                (join, second)[stage](0, progress[stage])
+                progress[stage] += 1
+
+        for h in range(count - 1):
+            i, p = divmod(h, parts_d)
+            if i > 0:
+                ended(2 + p, i - 1)
+            late_block(h)
+            to_core(0, h)
+            if h > 2:
+                catch_up(1, h - 3)
+            catch_up(0, h - 1)
+            if h == parts_d * (nz - 2) - 1:
+                catch_up(0, h)
+                catch_up(1, h - 1)
+        catch_up(0, count - 2)
+        catch_up(1, count - 4)
+        if nz > 1:
+            ended(1 + parts_d, nz - 2)
+        late_block(count - 1)
+        to_core(0, count - 1)
+
+    @pl.when(inside)
+    def _():
+        for h in range(count):
+            late_block(h)
+            to_core(0, h)
+            if h > 1:
+                join(0, h - 2)
+        for h in range(max(count - 2, 0), count - 1):
+            join(0, h)
+
+    def seconds_late(begin_at):
+        @pl.loop(begin_at, count)
+        def _(h):
+            second(0, h)
+
+    backward(0)
+    join(0, count - 1)
+    first_out()
     if nz > 2:
         chain(0)
-    step(nz - 1, 2)
-    if nz > 1:
-        ended(2, nz - 2)
-    late_block(nz - 1)
-    to_core(0, nz - 1)
-    backward(qd)
-    step(nz, 1)
-    early_out(qd, 0)
-    step(nz, 2)
-    backward(qa)
-    joins(0)
-    early_out(qa, 2)
-    backward(qb)
-    early_out(qb, 1)
-    step(nz + 1, 2)
-    joins(2)
+
+    @pl.when(at_end)
+    def _():
+        seconds_late(max(count - 3, 0))
+
+    @pl.when(inside)
+    def _():
+        seconds_late(0)
+
+    backward(1)
+    backward(2)
     for j in range(1, nz - 2):
         chain(j)
-    backward(q)
-    joins(1)
-    early_out(q, 3)
-    seconds()
+    pair_out()
     if nz > 1:
         hand_on()
+    for i in range(max(nz - 2, 0), nz):
+        second(1, i)
+    backward(3)
+    last_out()
+    joins(3)
+    if nz > 1:
         settle()
-    joins(3)
     finishes(0)
-    ended_out(0)
-    y_copy = pltpu.make_async_copy(y, y_out, loc.at[7])
-    y_copy.start()
     finishes(1)
     exchange(arrival)
     keep_own(z, hand)
@@ -573,9 +679,7 @@
                 out = out + e[sl, :].astype(jnp.float32)
             g[sl, :] = gd[sl, :] + out
 
-    inner = jnp.logical_and(first, last) if nz > 1 else low
-
-    @pl.when(inner)
+    @pl.when(inside)
     def _():
         grad_sum()
 
@@ -590,9 +694,8 @@
 
     g_copy = pltpu.make_async_copy(g, g_out, loc.at[8])
     g_copy.start()
-    ended_out(1)
-    dx_copy = pltpu.make_async_copy(dx, dx_out, loc.at[9])
-    dx_copy.start()
+    for t in range(2):
+        ended_out(t)
     for copies in (weights, near, far):
         for copy in copies.values():
             copy.wait_send()
@@ -600,15 +703,16 @@
         copy.wait_send()
     exchange(sent)
     for t in range(2):
-        @pl.loop(0, nz)
+        @pl.loop(0, blocks[t])
         def _(i, t=t):
             for n in range(4):
                 core_copy(t, i, n).wait_send()
             for slot in range(3):
                 plane_copy(t, i, slot).wait_send()
             end_copy(t, i).wait_send()
+            own_copy(t, i).wait()
     for s in range(nz - 1):
-        for k in range(3):
+        for k in range(2 + parts_d):
             onward(k, s, sent)
     for m in range(nz - 2):
         @pl.when(jnp.logical_and(last, z <= m))
@@ -628,8 +732,7 @@
         def _():
             leftward(0, nz - 2, sent)
 
-    for copy in (y_copy, g_copy, dx_copy):
-        copy.wait()
+    g_copy.wait()
 
 
 def layer(nz, xs, w_gate, w_up, w_down, taps, bias, grad_down):
@@ -642,16 +745,19 @@
     b16, f32 = jnp.bfloat16, jnp.float32
     out = jax.ShapeDtypeStruct((rows, d), b16)
     hops = max(nz - 1, 1)
+    parts_d = wide // 256 if wide % 256 == 0 else 1
+    count = nz * parts_d
     return pl.pallas_call(
         functools.partial(layer_kernel, nz, tile),
         out_shape=(out, out, jax.ShapeDtypeStruct((u * GROUP, r), f32)),
         in_specs=[ANY] * 6 + [VMEM] * 2 + [ANY],
         out_specs=(ANY,) * 3,
-        scratch_shapes=[pltpu.VMEM((rows, d), b16)] * 2
+        scratch_shapes=[pltpu.VMEM((half, d), b16)] * 2
         + [pltpu.VMEM((u * GROUP, r), f32)] * 2
         + [pltpu.VMEM((GROUP, rows, d), b16)] * 3
         + [pltpu.VMEM((d, u), b16)] * 2
         + [pltpu.VMEM((u, d), b16), pltpu.VMEM((toks, u), b16), pltpu.VMEM((u, toks), b16),
+           pltpu.VMEM((toks, u), f32), pltpu.VMEM((toks, u), f32),
            pltpu.VMEM((toks, u), f32), pltpu.VMEM((toks, u), f32),
            pltpu.VMEM((toks, u), b16), pltpu.VMEM((toks, u), b16),
            pltpu.VMEM((toks, d), b16), pltpu.VMEM((toks, d), b16), pltpu.VMEM((u, d), b16),
@@ -659,9 +765,10 @@
            pltpu.VMEM((hops, u, wide), b16), pltpu.VMEM((hops, u, wide), b16)]
         + [pltpu.VMEM((u * GROUP, r), b16)] * 3
         + [pltpu.SemaphoreType.DMA((10,))]
-        + sems(3, 3) + sems(3, 3) + sems(3, 3) + sems(hops, 3) + sems(hops, 3)
-        + sems(2, nz, 4) + sems(2, nz, 3) + sems(hops) + sems(hops) + sems(3)
-        + sems(3) + sems(3) + sems(1) + sems(1) + sems(2, nz),
+        + sems(3, 3) + sems(3, 3) + sems(3, 3) + sems(hops, 2 + parts_d) + sems(hops, 2 + parts_d)
+        + sems(2, count, 4) + sems(2, count, 3) + sems(hops) + sems(hops) + sems(3)
+        + sems(3) + sems(3) + sems(1) + sems(1) + sems(2, count)
+        + [pltpu.SemaphoreType.DMA((2, count))],
         compiler_params=pltpu.CompilerParams(collective_id=0, has_side_effects=True, vmem_limit_bytes=VMEM_BYTES),
         name="layer_group",
     )(*xs, w_gate, w_up, w_down, taps, bias, grad_down)
@@ -741,11 +848,45 @@
     return (y_late, dx_early, grad_down_out)
 
 
+def carry_kernel(pieces, *refs):
+    ins, outs, held, r_s, w_s = refs[:3], refs[3:6], refs[6:9], refs[9], refs[10]
+
+    def move(i, p, back):
+        rows = ins[i].shape[0] // pieces
+        sl = pl.ds(p * rows, rows)
+        src, dst = (held[i], outs[i]) if back else (ins[i], held[i])
+        return pltpu.make_async_copy(src.at[sl, :], dst.at[sl, :], (w_s if back else r_s).at[i, p])
+
+    steps = [(i, p) for i in range(3) for p in range(pieces)]
+    for i, p in steps:
+        move(i, p, False).start()
+    for i, p in steps:
+        move(i, p, False).wait()
+        move(i, p, True).start()
+    for i, p in steps:
+        move(i, p, True).wait()
+
+
+def carry(*arrays):
+    pieces = 2
+    return pl.pallas_call(
+        functools.partial(carry_kernel, pieces),
+        out_shape=tuple(jax.ShapeDtypeStruct(a.shape, a.dtype) for a in arrays),
+        in_specs=[ANY] * 3,
+        out_specs=(ANY,) * 3,
+        scratch_shapes=[pltpu.VMEM(a.shape, a.dtype) for a in arrays]
+        + [pltpu.SemaphoreType.DMA((3, pieces))] * 2,
+        compiler_params=pltpu.CompilerParams(vmem_limit_bytes=VMEM_BYTES),
+        name="results",
+    )(*arrays)
+
+
 def grouped_shards(nz, x_late, x_early, cotangent, w_gate, w_up, w_down, conv_taps, conv_bias, grad_down):
-    return layer(
+    outputs = layer(
         nz, (x_late, x_early, cotangent), w_gate, w_up, w_down, conv_taps,
         conv_bias.reshape(1, conv_bias.shape[0]), grad_down,
     )
+    return carry(*outputs)
 
 
 def solution(mesh):

time: 149 us -> 143 us (0.960)
  local copies, waits for them, and re-layouts: 4.97 us -> 0 us
    unnamed x7 -> x0, local copies, waits for them, and re-layouts: 4.97 us -> none
    pallas_call x1, Pallas kernels: 142 us -> 139 us  [layer(): pl.pallas_call(functools.partial(layer_kernel, nz, tile), out_shape=(out,...]
    pallas_call x0 -> x1, Pallas kernels: none -> 2.8 us  [carry(): pl.pallas_call(functools.partial(carry_kernel, pieces), out_shape=tuple((...]
where the time goes in v3:
time: 143 us
  Pallas kernels  142 us (99%)
    pallas_call x1, Pallas kernels, layer(): pl.pallas_call(functools.partial(layer_kernel, nz, tile), out_shape=(out,...  139 us

profile of v3, /device:TPU:0, one launch (start us, length us, event | category | flops | bytes accessed | tf_op | source)
XLA Modules:
  0.0 142.9 jit_solution(14476755002530930503)
XLA Ops:
  0.6 139.3 %layer_group.1 = (bf16[256,2048]{1,0:T(8,128)(2,1)}, bf16[256,2048]{1,0:T(8,128)(2,1)}, f32[2048,128]{1,0:T(8,128)}) custom-call(bf16[256,2048]{1,0:T(8,128)(2,1)} %x0.1, bf16[256,2048]{1,0:T(8,128)(2,1)} %x1.1, bf16[256,2048]{1,0:T(8,128)(2,1)} %x2.1, bf16[128,2048]{1,0:T(8,128)(2,1)} %wg.1, bf16[128,2048]{1,0:T(8,128)(2,1)} %wu.1, bf16[2048,128]{1,0:T(8,128)(2,1)} %wd.1, ...), custom_call_target="tpu_custom_call" | custom-call | tf_op jit(solution)/shard_map/layer_group/pallas_call | solution.py:750
  140.0 2.8 %results.1 = (bf16[256,2048]{1,0:T(8,128)(2,1)}, bf16[256,2048]{1,0:T(8,128)(2,1)}, f32[2048,128]{1,0:T(8,128)}) custom-call(bf16[256,2048]{1,0:T(8,128)(2,1)} %get-tuple-element.6.refs_0_, bf16[256,2048]{1,0:T(8,128)(2,1)} %get-tuple-element.7.refs_1_, f32[2048,128]{1,0:T(8,128)} %get-tuple-element.8.refs_2_), custom_call_target="tpu_custom_call" | custom-call | tf_op jit(solution)/shard_map/results/pallas_call | solution.py:872

commit v4 on v3

--- a/solution.py
+++ b/solution.py
@@ -275,45 +275,50 @@
             passing_l(arrival)
             passed_on_l().start()
 
-    def slot_r(o, m):
-        return remote(gp.at[:, at(o * wide, wide)], gin_r.at[m], zr_s.at[m], zr_r.at[m], fs=f + GROUP)
-
-    def slot_l(o, m):
-        return remote(gp.at[:, at(o * wide, wide)], gin_l.at[m], zl_s.at[m], zl_r.at[m], fs=f - GROUP)
-
-    def rightward(o, m, act=begin):
+    def slot_r(o, m, e):
+        there = gin_r.at[m, :, pl.ds(e * part, part)]
+        return remote(gp.at[:, at(o * wide + e * part, part)], there, zr_s.at[m, e], zr_r.at[m, e], fs=f + GROUP)
+
+    def slot_l(o, m, e):
+        there = gin_l.at[m, :, pl.ds(e * part, part)]
+        return remote(gp.at[:, at(o * wide + e * part, part)], there, zl_s.at[m, e], zl_r.at[m, e], fs=f - GROUP)
+
+    halves = range(parts_d)
+
+    def pass_part(o, into, send_sems, recv_sems, e):
+        for d, peer in enumerate((qa, qb, qd)):
+            @pl.when(lax.div(peer * r, part) == e)
+            def _(d=d, peer=peer):
+                src = gp.at[:, at(o * wide + peer * r, r)]
+                remote(src, into.at[at(q * u, u), :], send_sems.at[d], recv_sems.at[d], fs=base + peer).start()
+        if e == parts_d - 1:
+            keep_own(o, into)
+
+    def rightward(o, m, e):
         if m < nz - 2:
-            act(slot_r(o, m))
+            slot_r(o, m, e).start()
             return
 
         @pl.when(z == nz - 2)
         def _():
-            passing_r(act)
-            if act is begin:
-                keep_own(nz - 1, passed_r)
-            else:
-                act(passed_on_r())
+            pass_part(nz - 1, passed_r, pr_s, pr_r, e)
 
         @pl.when(z < nz - 2)
         def _():
-            act(slot_r(o, m))
-
-    def leftward(o, m, act=begin):
+            slot_r(o, m, e).start()
+
+    def leftward(o, m, e):
         if m < nz - 2:
-            act(slot_l(o, m))
+            slot_l(o, m, e).start()
             return
 
         @pl.when(z == 1)
         def _():
-            passing_l(act)
-            if act is begin:
-                keep_own(0, passed_l)
-            else:
-                act(passed_on_l())
+            pass_part(0, passed_l, pl_s, pl_r, e)
 
         @pl.when(z > 1)
         def _():
-            act(slot_l(o, m))
+            slot_l(o, m, e).start()
 
     def down_grad():
         for i in range(nz):
@@ -324,11 +329,13 @@
             if i < nz - 1:
                 @pl.when(low)
                 def _():
-                    rightward(o, i)
+                    for e in halves:
+                        rightward(o, i, e)
 
                 @pl.when(high)
                 def _():
-                    leftward(o, i)
+                    for e in halves:
+                        leftward(o, i, e)
 
         @pl.when(jnp.logical_or(low, high))
         def _():
@@ -338,30 +345,30 @@
         @pl.when(jnp.logical_and(first, last))
         def _():
             m = nz - 2
-            slot_r(z, m).wait_recv()
-            slot_l(z, m).wait_recv()
+            for e in halves:
+                slot_r(z, m, e).wait_recv()
+                slot_l(z, m, e).wait_recv()
             home = gp.at[:, at(z * wide, wide)]
             total(home, [home, gin_r.at[m], gin_l.at[m]], u)
             exchange(begin)
 
-    def chain(j):
-        o = nz - 2 + z - j
+    def chain(j, e):
+        o, p = nz - 2 + z - j, z + 2 - nz + j
+        here = pl.ds(e * part, part)
 
         @pl.when(jnp.logical_and(first, o <= nz - 1))
         def _():
-            slot_r(o, j).wait_recv()
-            cols = at(o * wide, wide)
-            total(gp.at[:, cols], [gp.at[:, cols], gin_r.at[j]], u)
-            rightward(o, j + 1)
-
-        p = z + 2 - nz + j
+            slot_r(o, j, e).wait_recv()
+            cols = at(o * wide + e * part, part)
+            total(gp.at[:, cols], [gp.at[:, cols], gin_r.at[j, :, here]], u)
+            rightward(o, j + 1, e)
 
         @pl.when(jnp.logical_and(last, p >= 0))
         def _():
-            slot_l(p, j).wait_recv()
-            cols = at(p * wide, wide)
-            total(gp.at[:, cols], [gp.at[:, cols], gin_l.at[j]], u)
-            leftward(p, j + 1)
+            slot_l(p, j, e).wait_recv()
+            cols = at(p * wide + e * part, part)
+            total(gp.at[:, cols], [gp.at[:, cols], gin_l.at[j, :, here]], u)
+            leftward(p, j + 1, e)
 
     def backward(n):
         b, out = order[n], pl.ds(n * rows, rows)
@@ -602,11 +609,11 @@
             if h > 2:
                 catch_up(1, h - 3)
             catch_up(0, h - 1)
-            if h == parts_d * (nz - 2) - 1:
+            if h in (parts_d * (nz - 2) - 1, parts_d * (nz - 1) - 1):
                 catch_up(0, h)
                 catch_up(1, h - 1)
         catch_up(0, count - 2)
-        catch_up(1, count - 4)
+        catch_up(1, count - 3)
         if nz > 1:
             ended(1 + parts_d, nz - 2)
         late_block(count - 1)
@@ -627,49 +634,8 @@
         def _(h):
             second(0, h)
 
-    backward(0)
-    join(0, count - 1)
-    first_out()
     if nz > 2:
-        chain(0)
-
-    @pl.when(at_end)
-    def _():
-        seconds_late(max(count - 3, 0))
-
-    @pl.when(inside)
-    def _():
-        seconds_late(0)
-
-    backward(1)
-    backward(2)
-    for j in range(1, nz - 2):
-        chain(j)
-    pair_out()
-    if nz > 1:
-        hand_on()
-    for i in range(max(nz - 2, 0), nz):
-        second(1, i)
-    backward(3)
-    last_out()
-    joins(3)
-    if nz > 1:
-        settle()
-    finishes(0)
-    finishes(1)
-    exchange(arrival)
-    keep_own(z, hand)
-    if nz > 1:
-        @pl.when(high)
-        def _():
-            passed_on_r().wait_recv()
-
-        @pl.when(low)
-        def _():
-            passed_on_l().wait_recv()
-
-    old_grad.wait()
-
+        chain(0, 0)
     def grad_sum(*extra):
         @pl.loop(0, GROUP * u, step=128)
         def _(i):
@@ -679,21 +645,73 @@
                 out = out + e[sl, :].astype(jnp.float32)
             g[sl, :] = gd[sl, :] + out
 
+    g_copy = pltpu.make_async_copy(g, g_out, loc.at[8])
+
+    def grad_out():
+        exchange(arrival)
+        keep_own(z, hand)
+        old_grad.wait()
+
+        @pl.when(inside)
+        def _():
+            grad_sum()
+
+        if nz > 1:
+            @pl.when(high)
+            def _():
+                passed_on_r().wait_recv()
+                grad_sum(passed_r)
+
+            @pl.when(low)
+            def _():
+                passed_on_l().wait_recv()
+                grad_sum(passed_l)
+
+        g_copy.start()
+
+    backward(0)
+    join(0, count - 1)
+    first_out()
+    for e in range(1, parts_d if nz > 2 else 0):
+        chain(0, e)
+
+    @pl.when(at_end)
+    def _():
+        seconds_late(max(count - 2, 0))
+
     @pl.when(inside)
     def _():
-        grad_sum()
-
+        seconds_late(0)
+
+    backward(1)
+    backward(2)
+    for j in range(1, nz - 2):
+        for e in halves:
+            chain(j, e)
+    pair_out()
     if nz > 1:
-        @pl.when(high)
-        def _():
-            grad_sum(passed_r)
-
-        @pl.when(low)
-        def _():
-            grad_sum(passed_l)
-
-    g_copy = pltpu.make_async_copy(g, g_out, loc.at[8])
-    g_copy.start()
+        hand_on()
+    for i in range(max(nz - 2, 0), nz):
+        second(1, i)
+    backward(3)
+    if nz > 1:
+        settle()
+    last_out()
+    joins(3)
+    finishes(0)
+
+    @pl.when(at_end)
+    def _():
+        for i in range(nz - 1):
+            finish(1, i)
+        grad_out()
+        finish(1, nz - 1)
+
+    @pl.when(inside)
+    def _():
+        finishes(1)
+        grad_out()
+
     for t in range(2):
         ended_out(t)
     for copies in (weights, near, far):
@@ -717,20 +735,34 @@
     for m in range(nz - 2):
         @pl.when(jnp.logical_and(last, z <= m))
         def _(m=m):
-            rightward(0, m, sent)
+            for e in halves:
+                slot_r(0, m, e).wait_send()
 
         @pl.when(jnp.logical_and(first, nz - 1 - z <= m))
         def _(m=m):
-            leftward(0, m, sent)
+            for e in halves:
+                slot_l(0, m, e).wait_send()
 
     if nz > 1:
-        @pl.when(last)
-        def _():
-            rightward(0, nz - 2, sent)
-
-        @pl.when(first)
-        def _():
-            leftward(0, nz - 2, sent)
+        @pl.when(z < nz - 2)
+        def _():
+            for e in halves:
+                slot_r(0, nz - 2, e).wait_send()
+
+        @pl.when(z == nz - 2)
+        def _():
+            passing_r(sent)
+            passed_on_r().wait_send()
+
+        @pl.when(z > 1)
+        def _():
+            for e in halves:
+                slot_l(0, nz - 2, e).wait_send()
+
+        @pl.when(z == 1)
+        def _():
+            passing_l(sent)
+            passed_on_l().wait_send()
 
     g_copy.wait()
 
@@ -766,7 +798,7 @@
         + [pltpu.VMEM((u * GROUP, r), b16)] * 3
         + [pltpu.SemaphoreType.DMA((10,))]
         + sems(3, 3) + sems(3, 3) + sems(3, 3) + sems(hops, 2 + parts_d) + sems(hops, 2 + parts_d)
-        + sems(2, count, 4) + sems(2, count, 3) + sems(hops) + sems(hops) + sems(3)
+        + sems(2, count, 4) + sems(2, count, 3) + sems(hops, parts_d) + sems(hops, parts_d) + sems(3)
         + sems(3) + sems(3) + sems(1) + sems(1) + sems(2, count)
         + [pltpu.SemaphoreType.DMA((2, count))],
         compiler_params=pltpu.CompilerParams(collective_id=0, has_side_effects=True, vmem_limit_bytes=VMEM_BYTES),

time: 143 us -> 143 us (level)
  no operation moved by 1% of the time
where the time goes in v4:
time: 143 us; the launch traced here: 142 us
  Pallas kernels  141 us (99%)
    pallas_call x1, Pallas kernels, layer(): pl.pallas_call(functools.partial(layer_kernel, nz, tile), out_shape=(out,...  139 us

profile of v4, /device:TPU:0, one launch (start us, length us, event | category | flops | bytes accessed | tf_op | source)
XLA Modules:
  0.0 142.2 jit_solution(14112260186771593659)
XLA Ops:
  0.6 138.6 %layer_group.1 = (bf16[256,2048]{1,0:T(8,128)(2,1)}, bf16[256,2048]{1,0:T(8,128)(2,1)}, f32[2048,128]{1,0:T(8,128)}) custom-call(bf16[256,2048]{1,0:T(8,128)(2,1)} %x0.1, bf16[256,2048]{1,0:T(8,128)(2,1)} %x1.1, bf16[256,2048]{1,0:T(8,128)(2,1)} %x2.1, bf16[128,2048]{1,0:T(8,128)(2,1)} %wg.1, bf16[128,2048]{1,0:T(8,128)(2,1)} %wu.1, bf16[2048,128]{1,0:T(8,128)(2,1)} %wd.1, ...), custom_call_target="tpu_custom_call" | custom-call | tf_op jit(solution)/shard_map/layer_group/pallas_call | solution.py:782
  139.3 2.8 %results.1 = (bf16[256,2048]{1,0:T(8,128)(2,1)}, bf16[256,2048]{1,0:T(8,128)(2,1)}, f32[2048,128]{1,0:T(8,128)}) custom-call(bf16[256,2048]{1,0:T(8,128)(2,1)} %get-tuple-element.6.refs_0_, bf16[256,2048]{1,0:T(8,128)(2,1)} %get-tuple-element.7.refs_1_, f32[2048,128]{1,0:T(8,128)} %get-tuple-element.8.refs_2_), custom_call_target="tpu_custom_call" | custom-call | tf_op jit(solution)/shard_map/results/pallas_call | solution.py:904

commit v5 on v4

--- a/solution.py
+++ b/solution.py
@@ -699,39 +699,22 @@
     last_out()
     joins(3)
     finishes(0)
-
-    @pl.when(at_end)
-    def _():
-        for i in range(nz - 1):
-            finish(1, i)
-        grad_out()
-        finish(1, nz - 1)
-
-    @pl.when(inside)
-    def _():
-        finishes(1)
-        grad_out()
-
-    for t in range(2):
-        ended_out(t)
     for copies in (weights, near, far):
         for copy in copies.values():
             copy.wait_send()
     for copy in partner:
         copy.wait_send()
-    exchange(sent)
-    for t in range(2):
-        @pl.loop(0, blocks[t])
-        def _(i, t=t):
-            for n in range(4):
-                core_copy(t, i, n).wait_send()
-            for slot in range(3):
-                plane_copy(t, i, slot).wait_send()
-            end_copy(t, i).wait_send()
-            own_copy(t, i).wait()
     for s in range(nz - 1):
         for k in range(2 + parts_d):
             onward(k, s, sent)
+
+    @pl.loop(0, count)
+    def _(i):
+        for n in range(4):
+            core_copy(0, i, n).wait_send()
+        for slot in range(3):
+            plane_copy(0, i, slot).wait_send()
+
     for m in range(nz - 2):
         @pl.when(jnp.logical_and(last, z <= m))
         def _(m=m):
@@ -752,7 +735,6 @@
         @pl.when(z == nz - 2)
         def _():
             passing_r(sent)
-            passed_on_r().wait_send()
 
         @pl.when(z > 1)
         def _():
@@ -762,6 +744,52 @@
         @pl.when(z == 1)
         def _():
             passing_l(sent)
+
+    def settled():
+        ended_out(0)
+
+        @pl.loop(0, count)
+        def _(i):
+            end_copy(0, i).wait_send()
+            own_copy(0, i).wait()
+
+        @pl.loop(0, nz)
+        def _(i):
+            for n in range(4):
+                core_copy(1, i, n).wait_send()
+            for slot in range(2):
+                plane_copy(1, i, slot).wait_send()
+
+    @pl.when(at_end)
+    def _():
+        for i in range(nz - 1):
+            finish(1, i)
+        settled()
+        grad_out()
+        finish(1, nz - 1)
+
+    @pl.when(inside)
+    def _():
+        finishes(1)
+        settled()
+        grad_out()
+
+    ended_out(1)
+    exchange(sent)
+
+    @pl.loop(0, nz)
+    def _(i):
+        plane_copy(1, i, 2).wait_send()
+        end_copy(1, i).wait_send()
+        own_copy(1, i).wait()
+
+    if nz > 1:
+        @pl.when(z == nz - 2)
+        def _():
+            passed_on_r().wait_send()
+
+        @pl.when(z == 1)
+        def _():
             passed_on_l().wait_send()
 
     g_copy.wait()

time: 143 us -> 142 us (level)
  no operation moved by 1% of the time
where the time goes in v5:
time: 142 us
  Pallas kernels  141 us (99%)
    pallas_call x1, Pallas kernels, layer(): pl.pallas_call(functools.partial(layer_kernel, nz, tile), out_shape=(out,...  139 us

profile of v5, /device:TPU:0, one launch (start us, length us, event | category | flops | bytes accessed | tf_op | source)
XLA Modules:
  0.0 142.2 jit_solution(16412200020500627380)
XLA Ops:
  0.6 138.6 %layer_group.1 = (bf16[256,2048]{1,0:T(8,128)(2,1)}, bf16[256,2048]{1,0:T(8,128)(2,1)}, f32[2048,128]{1,0:T(8,128)}) custom-call(bf16[256,2048]{1,0:T(8,128)(2,1)} %x0.1, bf16[256,2048]{1,0:T(8,128)(2,1)} %x1.1, bf16[256,2048]{1,0:T(8,128)(2,1)} %x2.1, bf16[128,2048]{1,0:T(8,128)(2,1)} %wg.1, bf16[128,2048]{1,0:T(8,128)(2,1)} %wu.1, bf16[2048,128]{1,0:T(8,128)(2,1)} %wd.1, ...), custom_call_target="tpu_custom_call" | custom-call | tf_op jit(solution)/shard_map/layer_group/pallas_call | solution.py:810
  139.2 2.8 %results.1 = (bf16[256,2048]{1,0:T(8,128)(2,1)}, bf16[256,2048]{1,0:T(8,128)(2,1)}, f32[2048,128]{1,0:T(8,128)}) custom-call(bf16[256,2048]{1,0:T(8,128)(2,1)} %get-tuple-element.6.refs_0_, bf16[256,2048]{1,0:T(8,128)(2,1)} %get-tuple-element.7.refs_1_, f32[2048,128]{1,0:T(8,128)} %get-tuple-element.8.refs_2_), custom_call_target="tpu_custom_call" | custom-call | tf_op jit(solution)/shard_map/results/pallas_call | solution.py:932
